TPU v7x, 256 devices: a whole 4x4x8 slice. The times are simulated.
256 devices in a mesh: kv: 32 (over z, x), tp: 8 (over y, core).
Axes of the slice: x: 4, y: 4, z: 8, core: 2. Of those that a mesh axis runs over, the one named last changes fastest.
Arguments:
- tokens: bfloat16 [1024, 4096], P('kv', 'tp'), may hold values from -12 to 12
- norm_gain: float32 [4096], replicated, may hold values from 0.1 to 1.9
- query_weight: bfloat16 [4096, 4096], P('kv', 'tp'), may hold values from -0.09375 to 0.09375
- key_weight: bfloat16 [4096, 4096], P('kv', 'tp'), may hold values from -0.09375 to 0.09375
- value_weight: bfloat16 [4096, 4096], P('kv', 'tp'), may hold values from -0.09375 to 0.09375
- outgate_weight: bfloat16 [4096, 4096], P('kv', 'tp'), may hold values from -0.09375 to 0.09375
- ingate_weight: bfloat16 [4096, 16], replicated, may hold values from -0.09375 to 0.09375
- forget_weight: bfloat16 [4096, 16], replicated, may hold values from -0.09375 to 0.09375
- forget_bias: float32 [16], replicated, may hold values from 0.5 to 4
- output_weight: bfloat16 [4096, 4096], P('tp', 'kv'), may hold values from -0.09375 to 0.09375
- state_memory: float32 [256, 16, 256, 256], P('kv', 'tp'), may hold values from -0.8 to 0.8
- state_normaliser: float32 [256, 16, 256], P('kv', 'tp'), may hold values from -0.8 to 0.8
- state_stabiliser: float32 [256, 16], P('kv', 'tp'), may hold values from -4 to 4
- past_keys: bfloat16 [256, 4, 4096], P('kv', None, 'tp'), may hold values from -6 to 6
- past_values: bfloat16 [256, 4, 4096], P('kv', None, 'tp'), may hold values from -6 to 6
- past_ingate: float32 [256, 4, 16], P('kv', None, 'tp'), may hold values from -4 to 4
- past_forget: float32 [256, 4, 16], P('kv', None, 'tp'), may hold values from -1 to 4
- accepted: int32 [256], P('kv'), may hold values from 0 to 4
Outputs:
- mixed: bfloat16 [1024, 4096], P('kv', 'tp')
- taken_memory: float32 [256, 16, 256, 256], P('kv', 'tp')
- taken_normaliser: float32 [256, 16, 256], P('kv', 'tp')
- taken_stabiliser: float32 [256, 16], P('kv', 'tp')
- new_keys: bfloat16 [1024, 4096], P('kv', 'tp')
- new_values: bfloat16 [1024, 4096], P('kv', 'tp')
All inputs are finite; a program needn't handle non-finite values.
Results may differ from a plain program's by a relative error of at most 0.03.
Values may be sent and summed in bfloat16 or wider, within the bound.
A program may use at most 64 MiB of HBM per device.

v0:
```python
import jax
import jax.numpy as jnp
from jax import lax
from jax.sharding import Mesh
from jax.sharding import PartitionSpec as P

D = 4096
DK = 256
KV = ("kv_0", "kv_1")


epsilon = 1e-06


def laid_out(parts, dim):
    parts = jnp.moveaxis(parts, 0, dim)
    dims = parts.shape
    return parts.reshape(*dims[:dim], dims[dim] * dims[dim + 1], *dims[dim + 2 :])


def from_everyone(x, axis):
    devices = lax.axis_size(axis)
    return lax.all_to_all(jnp.broadcast_to(x[None], (devices, *x.shape)), axis, 0, 0, tiled=True)


def gathered_copies(x, axis, dim):
    return laid_out(from_everyone(x, axis), dim)


def of_everyone(x, axis):
    return from_everyone(x, axis).sum(axis=0)


def summed_rows(terms, axes):
    so_far = terms.astype(jnp.bfloat16)
    for axis in axes:
        so_far = lax.psum_scatter(so_far, axis, scatter_dimension=0, tiled=True)
    return so_far.astype(jnp.float32)


def gathered_by_axis(x, axes, dim):
    if not axes:
        return x
    nearer = lax.all_gather(x, axes[-1], axis=dim, tiled=True)
    return gathered_by_axis(nearer, axes[:-1], dim)


def split_up(x, dim, devices):
    dims = x.shape
    parts = x.reshape(*dims[:dim], devices, dims[dim] // devices, *dims[dim + 1 :])
    return jnp.moveaxis(parts, dim, 0)


def summed_on_arrival(x, axis, dim):
    devices = lax.axis_size(axis)
    parts = lax.all_to_all(split_up(x, dim, devices), axis, 0, 0, tiled=True)
    return jnp.sum(parts.astype(jnp.float32), axis=0)


def rounded(values):
    return lax.optimization_barrier(values.astype(jnp.bfloat16))


def heads_view(rows, seq_count, head_count):
    shaped = rows.astype(jnp.float32).reshape(
        seq_count, -1, head_count, rows.shape[-1] // head_count
    )
    return shaped.transpose(0, 2, 1, 3)


def catch_up(memory, normaliser, stabiliser, key_rows, values, in_gate, forget_pre, taken_mask):
    log_forget = jnp.where(taken_mask, jax.nn.log_sigmoid(forget_pre), 0.0)
    running = jnp.cumsum(log_forget, axis=-1)
    chain_total = running[..., -1]
    end_logs = jnp.where(taken_mask, chain_total[..., None] - running + in_gate, -jnp.inf)
    stable_new = jnp.maximum(chain_total + stabiliser, jnp.max(end_logs, axis=-1))
    carry_decay = jnp.exp(chain_total + stabiliser - stable_new)
    weighted = key_rows * jnp.exp(end_logs - stable_new[..., None])[..., None]
    memory_new = carry_decay[..., None, None] * memory + jnp.einsum(
        "...pd,...pe->...de", weighted, values
    )
    normaliser_new = carry_decay[..., None] * normaliser + jnp.sum(weighted, axis=-2)
    return (memory_new, normaliser_new, stable_new)


def advance(memory, normaliser, stabiliser, query_rows, key_rows, values, in_gate, forget_pre):
    chain_len = query_rows.shape[-2]
    running = jnp.cumsum(jax.nn.log_sigmoid(forget_pre), axis=-1)
    causal = jnp.arange(chain_len)[:, None] >= jnp.arange(chain_len)[None, :]
    within = jnp.where(
        causal, running[..., :, None] - running[..., None, :] + in_gate[..., None, :], -jnp.inf
    )
    carried = running + stabiliser[..., None]
    stable = jnp.maximum(carried, jnp.max(within, axis=-1))
    scores = jnp.einsum("...td,...sd->...ts", query_rows, key_rows) * jnp.exp(
        within - stable[..., None]
    )
    carry_weight = jnp.exp(carried - stable)
    numerator = carry_weight[..., None] * jnp.einsum("...td,...de->...te", query_rows, memory)
    numerator = numerator + jnp.einsum("...ts,...se->...te", scores, values)
    denominator = carry_weight * jnp.einsum("...td,...d->...t", query_rows, normaliser) + jnp.sum(
        scores, axis=-1
    )
    return numerator / jnp.maximum(jnp.abs(denominator), 1.0)[..., None]


def body(
    tokens,
    norm_gain,
    query_weight,
    key_weight,
    value_weight,
    outgate_weight,
    ingate_weight,
    forget_weight,
    forget_bias,
    output_weight,
    state_memory,
    state_normaliser,
    state_stabiliser,
    past_keys,
    past_values,
    past_ingate,
    past_forget,
    accepted,
):
    seq_count, head_count = state_stabiliser.shape
    tok_rows = tokens.shape[0]
    chain_len = past_keys.shape[1]
    full_rows = gathered_copies(tokens, "tp", 1)
    own_part = tokens.astype(jnp.float32)
    squares = of_everyone(jnp.sum(own_part * own_part, axis=1, keepdims=True), "tp")
    normed = (full_rows.astype(jnp.float32) * lax.rsqrt(squares / D + epsilon) * norm_gain).astype(
        jnp.bfloat16
    )
    blocks = lax.all_to_all(normed, KV, split_axis=1, concat_axis=0, tiled=True)
    summed = summed_rows(
        jnp.concatenate(
            [
                jnp.dot(blocks, weight, preferred_element_type=jnp.float32)
                for weight in (query_weight, key_weight, value_weight, outgate_weight)
            ],
            axis=1,
        ),
        KV,
    )
    query_rows, key_rows, value_rows, out_pre = jnp.split(summed, 4, axis=1)
    query_b = rounded(query_rows)
    key_b = rounded(key_rows)
    value_b = rounded(value_rows)
    outgate_b = rounded(out_pre)
    first_head = lax.axis_index("tp") * head_count
    in_cols = lax.dynamic_slice_in_dim(ingate_weight, first_head, head_count, 1)
    forget_cols = lax.dynamic_slice_in_dim(forget_weight, first_head, head_count, 1)
    bias_own = lax.dynamic_slice_in_dim(forget_bias, first_head, head_count, 0)
    in_gate = jnp.dot(normed, in_cols, preferred_element_type=jnp.float32)
    forget_pre = jnp.dot(normed, forget_cols, preferred_element_type=jnp.float32) + bias_own
    key_scale = DK ** (-0.5)
    taken_mask = jnp.arange(chain_len)[None, None, :] < accepted[:, None, None]
    memory, normaliser, stabiliser = catch_up(
        state_memory,
        state_normaliser,
        state_stabiliser,
        heads_view(past_keys, seq_count, head_count) * key_scale,
        heads_view(past_values, seq_count, head_count),
        past_ingate.transpose(0, 2, 1),
        past_forget.transpose(0, 2, 1),
        taken_mask,
    )
    hidden = advance(
        memory,
        normaliser,
        stabiliser,
        heads_view(query_b, seq_count, head_count),
        heads_view(key_b, seq_count, head_count) * key_scale,
        heads_view(value_b, seq_count, head_count),
        in_gate.reshape(seq_count, chain_len, head_count).transpose(0, 2, 1),
        forget_pre.reshape(seq_count, chain_len, head_count).transpose(0, 2, 1),
    )
    gated_heads = jax.nn.sigmoid(heads_view(outgate_b, seq_count, head_count)) * hidden
    gated_rows = gated_heads.transpose(0, 2, 1, 3).reshape(tok_rows, -1).astype(jnp.bfloat16)
    partial_out = jnp.dot(
        gated_rows, gathered_by_axis(output_weight, KV, 1), preferred_element_type=jnp.float32
    )
    result = summed_on_arrival(partial_out.astype(jnp.bfloat16), "tp", 1).astype(jnp.bfloat16)
    return (result, memory, normaliser, stabiliser, key_b, value_b)


def solution(mesh):
    torus = Mesh(mesh.devices.reshape(8, 4, mesh.shape["tp"]), ("kv_0", "kv_1", "tp"))
    in_specs = (
        P(KV, "tp"),
        P(),
        P(KV, "tp"),
        P(KV, "tp"),
        P(KV, "tp"),
        P(KV, "tp"),
        P(),
        P(),
        P(),
        P("tp", KV),
        P(KV, "tp", None, None),
        P(KV, "tp", None),
        P(KV, "tp"),
        P(KV, None, "tp"),
        P(KV, None, "tp"),
        P(KV, None, "tp"),
        P(KV, None, "tp"),
        P(KV),
    )
    out_specs = (
        P(KV, "tp"),
        P(KV, "tp", None, None),
        P(KV, "tp", None),
        P(KV, "tp"),
        P(KV, "tp"),
        P(KV, "tp"),
    )
    return jax.shard_map(body, mesh=torus, in_specs=in_specs, out_specs=out_specs, check_vma=False)
```

profile of v0, /device:TPU:22, one launch (start us, length us, event | category | flops | bytes accessed | tf_op | source)
XLA Modules:
  0.0 214.9 jit_solution(11590030829380537056)
XLA Ops:
  7.2 0.9 multiply_reduce_fusion
  8.1 7.5 %all_to_all.31 = f32[8,32,1]{1,2,0:T(1,128)S(1)} all-to-all(f32[8,32,1]{1,2,0:T(1,128)S(1)} %broadcast_in_dim.27), channel_id=1, replica_groups=mesh['kv_0'=8,'kv_1'=4,'tp'=8] {'tp'}, dimensions={0} | all-to-all | bytes 2048 | tf_op jit(solution)/shard_map/all_to_all | solution.py:23
  15.7 1.5 broadcast_in_dim.26
  17.1 5.7 %all-to-all-start = ((bf16[8,32,512]{2,1,0:T(8,128)(2,1)}), bf16[8,32,512]{2,1,0:T(8,128)(2,1)S(1)}, u32[]{:S(2)}, u32[]{:S(2)}) async-start(bf16[8,32,512]{2,1,0:T(8,128)(2,1)} %broadcast_in_dim.26), calls=%async_computation | async-start | bytes 524288 | tf_op jit(solution)/shard_map/all_to_all | solution.py:23
  22.9 4.3 %all-to-all-done = bf16[8,32,512]{2,1,0:T(8,128)(2,1)S(1)} async-done(((bf16[8,32,512]{2,1,0:T(8,128)(2,1)}), bf16[8,32,512]{2,1,0:T(8,128)(2,1)S(1)}, u32[]{:S(2)}, u32[]{:S(2)}) %all-to-all-start) | async-done | bytes 262176 | tf_op jit(solution)/shard_map/all_to_all | solution.py:23
  27.9 22.6 %all_to_all.32 = bf16[32,32,128]{2,0,1:T(8,128)(2,1)S(1)} all-to-all(bf16[32,32,128]{2,0,1:T(8,128)(2,1)S(1)} %copy.130), channel_id=1, replica_groups=mesh['kv_0'=8,'kv_1'=4,'tp'=8] {'kv_0','kv_1'}, dimensions={1} | all-to-all | bytes 524288 | tf_op jit(solution)/shard_map/all_to_all | solution.py:136
  50.5 0.5 convolution_convert_fusion.1
  51.0 0.5 convolution_convert_fusion.2
  51.5 0.5 convolution_convert_fusion.3
  52.0 0.5 convolution_convert_fusion.4
  52.5 2.3 %pad_maximum_fusion = bf16[1024,2048]{0,1:T(8,128)(2,1)} fusion(bf16[1024,512]{0,1:T(8,128)(2,1)S(1)} %convolution_convert_fusion.1, bf16[1024,512]{0,1:T(8,128)(2,1)S(1)} %convolution_convert_fusion.2, bf16[1024,512]{0,1:T(8,128)(2,1)S(1)} %convolution_convert_fusion.3, bf16[1024,512]{0,1:T(8,128)(2,1)S(1)} %convolution_convert_fusion.4), kind=kLoop, calls=%fused_computation.1 | loop fusion | flops 16777216 | bytes 8388608 | tf_op jit(solution)/shard_map/concatenate | solution.py:138
  54.8 6.5 %copy.168 = bf16[1024,2048]{1,0:T(8,128)(2,1)} copy(bf16[1024,2048]{0,1:T(8,128)(2,1)} %pad_maximum_fusion) | data formatting | bytes 8388608
  61.4 52.5 %reduce-scatter.7.cloned.1.call-done = bf16[128,2048]{1,0:T(8,128)(2,1)} async-done(((bf16[1024,2048]{1,0:T(8,128)(2,1)}), bf16[128,2048]{1,0:T(8,128)(2,1)}) %reduce-scatter.7.cloned.1.call-update) | async-done | bytes 524304
  114.1 14.4 %all_gather.6 = bf16[512,512]{1,0:T(8,128)(2,1)} all-gather(bf16[512,128]{1,0:T(8,128)(2,1)S(1)} %copy-done.2), channel_id=1, replica_groups=mesh['kv_0'=8,'kv_1'=4,'tp'=8] {'kv_1'}, dimensions={1}, use_global_device_ids=true | all-gather | bytes 655360 | tf_op jit(solution)/shard_map/all_gather | solution.py:44
  129.2 0.4 reshape.144
  129.6 1.1 fusion.5
  131.0 2.2 %convolution_bitcast_fusion.2 = f32[8,2,4]{2,1,0:T(2,128)S(1)} fusion(f32[8,4,4096]{2,1,0:T(4,128)S(1)} %reshape.144, f32[4096]{0:T(1024)S(1)} %copy-done.8, f32[8,4]{1,0:T(8,128)S(1)} %rsqrt.13, bf16[4096,16]{0,1:T(8,128)(2,1)} %param.24, s32[]{:T(128)S(6)} %select_n.24), kind=kOutput, calls=%fused_computation.15 | convolution fusion | flops 917504 | bytes 557444 | tf_op jit(solution)/shard_map/dot_general | solution.py:156
  133.8 5.6 %multiply_add_fusion = f32[8,2,256,256]{3,2,1,0:T(8,128)} fusion(f32[8,2,256,256]{3,2,1,0:T(8,128)} %param.28, bf16[8,2,4,256]{3,2,1,0:T(4,128)(2,1)S(1)} %bitcast.145, f32[8,2]{1,0:T(8,128)S(1)} %get-tuple-element.38, bf16[8,4,2,256]{3,1,2,0:T(4,128)(2,1)S(1)} %bitcast.138, f32[8,2,4]{2,1,0:T(2,128)S(1)} %copy.147), kind=kOutput, calls=%fused_computation.2 | convolution fusion | flops 10518528 | bytes 8454464 | tf_op jit(solution)/shard_map/...pd,...pe->...de/dot_general | solution.py:79
  139.4 0.8 fusion.43
  141.6 2.5 %fusion.3 = f32[8,4,2,256]{3,1,2,0:T(4,128)S(1)} fusion(f32[8,2,256,256]{3,2,1,0:T(8,128)} %multiply_add_fusion, f32[8,4,2]{1,2,0:T(2,128)S(1)} %copy.144, bf16[8,2,4,256]{3,1,2,0:T(2,128)(2,1)S(1)} %bitcast.141), kind=kOutput, calls=%fused_computation.12 | convolution fusion | flops 8404992 | bytes 4292864 | tf_op jit(solution)/shard_map/...td,...de->...te/dot_general | solution.py:99
  144.4 51.2 %all-gather.2.cloned.1.call-done = bf16[512,4096]{1,0:T(8,128)(2,1)} async-done(((bf16[512,512]{1,0:T(8,128)(2,1)}), bf16[512,4096]{1,0:T(8,128)(2,1)}) %all-gather.2.cloned.1.call-update) | async-done | bytes 4194320 | tf_op jit(solution)/shard_map/all_gather | solution.py:44
  195.7 3.0 %convolution_convert_fusion = bf16[32,4096]{1,0:T(8,128)(2,1)S(1)} fusion(bf16[32,512]{1,0:T(8,128)(2,1)S(1)} %bitcast.142, bf16[512,4096]{1,0:T(8,128)(2,1)} %all-gather.2.cloned.1.call-done), kind=kOutput, calls=%fused_computation | convolution fusion | flops 134348800 | bytes 4489216 | tf_op jit(solution)/shard_map/dot_general | solution.py:182
  198.8 9.0 %all_to_all.33 = bf16[8,32,512]{2,1,0:T(8,128)(2,1)S(1)} all-to-all(bf16[8,32,512]{2,1,0:T(8,128)(2,1)S(1)} %bitcast.136), channel_id=1, replica_groups=mesh['kv_0'=8,'kv_1'=4,'tp'=8] {'tp'}, dimensions={0} | all-to-all | bytes 524288 | tf_op jit(solution)/shard_map/all_to_all | solution.py:56
  207.7 0.7 reduce_sum.55
  (98 shorter events, 4.0 us)
Async XLA Ops:
  7.2 43.4 %copy-start = (bf16[128,512]{1,0:T(8,128)(2,1)S(1)}, bf16[128,512]{1,0:T(8,128)(2,1)}, u32[]{:S(2)}) copy-start(bf16[128,512]{1,0:T(8,128)(2,1)} %param.23) | copy-start | bytes 393220
  7.2 20.5 %copy-start.8 = (f32[4096]{0:T(1024)S(1)}, f32[4096]{0:T(1024)}, u32[]{:S(2)}) copy-start(f32[4096]{0:T(1024)} %param.19) | copy-start | bytes 49156
  7.2 43.8 %copy-start.5 = (bf16[128,512]{1,0:T(8,128)(2,1)S(1)}, bf16[128,512]{1,0:T(8,128)(2,1)}, u32[]{:S(2)}) copy-start(bf16[128,512]{1,0:T(8,128)(2,1)} %param.22) | copy-start | bytes 393220
  17.1 10.1 %all-to-all-start = ((bf16[8,32,512]{2,1,0:T(8,128)(2,1)}), bf16[8,32,512]{2,1,0:T(8,128)(2,1)S(1)}, u32[]{:S(2)}, u32[]{:S(2)}) async-start(bf16[8,32,512]{2,1,0:T(8,128)(2,1)} %broadcast_in_dim.26), calls=%async_computation | async-start | bytes 524288 | tf_op jit(solution)/shard_map/all_to_all | solution.py:23
  22.8 28.7 %copy-start.6 = (bf16[128,512]{1,0:T(8,128)(2,1)S(1)}, bf16[128,512]{1,0:T(8,128)(2,1)}, u32[]{:S(2)}) copy-start(bf16[128,512]{1,0:T(8,128)(2,1)} %param.21) | copy-start | bytes 393220
  22.8 91.1 %reduce-scatter.7.cloned.1.call-start = ((), (), s32[]{:S(2)}) async-start(), calls=%async_computation.7 | async-start | bytes 4718592
  27.3 24.7 %copy-start.7 = (bf16[128,512]{1,0:T(8,128)(2,1)S(1)}, bf16[128,512]{1,0:T(8,128)(2,1)}, u32[]{:S(2)}) copy-start(bf16[128,512]{1,0:T(8,128)(2,1)} %param.20) | copy-start | bytes 393220
  61.3 52.8 %copy-start.2 = (bf16[512,128]{1,0:T(8,128)(2,1)S(1)}, bf16[512,128]{1,0:T(8,128)(2,1)}, u32[]{:S(2)}) copy-start(bf16[512,128]{1,0:T(8,128)(2,1)} %param.27) | copy-start | bytes 393220
  61.3 67.2 %copy-start.16 = (s32[8]{0:T(128)S(1)}, s32[8]{0:T(128)}, u32[]{:S(2)}) copy-start(s32[8]{0:T(128)} %param.35) | copy-start | bytes 100
  61.3 67.2 %copy-start.14 = (f32[8,4,2]{0,2,1:T(2,128)S(1)}, f32[8,4,2]{0,2,1:T(2,128)}, u32[]{:S(2)}) copy-start(f32[8,4,2]{0,2,1:T(2,128)} %param.34) | copy-start | bytes 772
  61.3 67.4 %copy-start.12 = (f32[8,4,2]{0,2,1:T(2,128)S(1)}, f32[8,4,2]{0,2,1:T(2,128)}, u32[]{:S(2)}) copy-start(f32[8,4,2]{0,2,1:T(2,128)} %param.33) | copy-start | bytes 772
  61.3 67.5 %copy-start.15 = (f32[8,2]{0,1:T(2,128)S(1)}, f32[8,2]{0,1:T(2,128)}, u32[]{:S(2)}) copy-start(f32[8,2]{0,1:T(2,128)} %param.30) | copy-start | bytes 196
  61.3 67.7 %copy-start.17 = (f32[16]{0:T(128)S(1)}, f32[16]{0:T(128)}, u32[]{:S(2)}) copy-start(f32[16]{0:T(128)} %param.26) | copy-start | bytes 196
  61.3 72.3 %copy-start.1 = (bf16[8,4,512]{2,1,0:T(4,128)(2,1)S(1)}, bf16[8,4,512]{2,1,0:T(4,128)(2,1)}, u32[]{:S(2)}) copy-start(bf16[8,4,512]{2,1,0:T(4,128)(2,1)} %param.31) | copy-start | bytes 98308
  61.4 72.4 %copy-start.10 = (f32[8,2,256]{2,1,0:T(2,128)S(1)}, f32[8,2,256]{2,1,0:T(2,128)}, u32[]{:S(2)}) copy-start(f32[8,2,256]{2,1,0:T(2,128)} %param.29) | copy-start | bytes 49156
  61.4 72.5 %copy-start.9 = (bf16[8,4,512]{2,1,0:T(4,128)(2,1)S(1)}, bf16[8,4,512]{2,1,0:T(4,128)(2,1)}, u32[]{:S(2)}) copy-start(bf16[8,4,512]{2,1,0:T(4,128)(2,1)} %param.32) | copy-start | bytes 98308
  61.4 78.0 %reduce-scatter.9.cloned.1.call-start = ((), (), s32[]{:S(2)}) async-start(), calls=%async_computation.8 | async-start | bytes 655360 | tf_op jit(solution)/shard_map/reduce_scatter | solution.py:37
  114.0 81.7 %all-gather.2.cloned.1.call-start = ((), (), s32[]{:S(2)}) async-start(), calls=%async_computation.6 | async-start | bytes 4718592 | tf_op jit(solution)/shard_map/all_gather | solution.py:44
  129.0 12.0 %copy-start.13 = (f32[8,2]{0,1:T(2,128)}, f32[8,2]{0,1:T(2,128)S(1)}, u32[]{:S(2)}) copy-start(f32[8,2]{0,1:T(2,128)S(1)} %copy.139) | copy-start | bytes 196
  133.8 7.0 %copy-start.11 = (f32[8,2,256]{2,1,0:T(2,128)}, f32[8,2,256]{2,1,0:T(2,128)S(1)}, u32[]{:S(2)}) copy-start(f32[8,2,256]{2,1,0:T(2,128)S(1)} %multiply_add_fusion.1) | copy-start | bytes 49156
  140.3 58.4 %copy-start.4 = (bf16[32,512]{1,0:T(8,128)(2,1)}, bf16[32,512]{1,0:T(8,128)(2,1)S(1)}, u32[]{:S(2)}) copy-start(bf16[32,512]{1,0:T(8,128)(2,1)S(1)} %get-tuple-element.44) | copy-start | bytes 98308
  141.5 57.2 %copy-start.3 = (bf16[32,512]{1,0:T(8,128)(2,1)}, bf16[32,512]{1,0:T(8,128)(2,1)S(1)}, u32[]{:S(2)}) copy-start(bf16[32,512]{1,0:T(8,128)(2,1)S(1)} %copy.155) | copy-start | bytes 98308
Sparse Core Ops, SparseCore 0:
  61.5 52.4 reduce-scatter.6
  116.5 20.9 reduce-scatter.8
  139.3 56.3 all-gather.1
where the time goes:
time: 219 us; the launch traced here: 215 us
  waiting for transfers between devices  108 us (49%)
  blocking collectives  53.6 us (24%)
  matrix products  16.9 us (8%)
  between operations  14.2 us (6%)
  local copies, waits for them, and re-layouts  11.7 us (5%)
  starting transfers between devices  5.79 us (3%)
  other arithmetic  4.66 us (2%)
    unnamed x4, waiting for transfers between devices  52.6 us
    all_gather x1, waiting for transfers between devices, gathered_by_axis(): nearer = lax.all_gather(x, axes[-1], axis=dim, tiled=True)  51.2 us
    all_to_all x1, blocking collectives, body(): blocks = lax.all_to_all(normed, KV, split_axis=1, concat_axis=0, tiled=True)  22.6 us
    all_gather x1, blocking collectives, gathered_by_axis(): nearer = lax.all_gather(x, axes[-1], axis=dim, tiled=True)  14.4 us
    all_to_all x1, blocking collectives, summed_on_arrival(): parts = lax.all_to_all(split_up(x, dim, devices), axis, 0, 0, tiled=True)  8.97 us
    all_to_all x1, blocking collectives, from_everyone(): lax.all_to_all(jnp.broadcast_to(x[None], (devices, *x.shape)), axis, 0, 0...  7.53 us
    unnamed x42, local copies, waits for them, and re-layouts  7.06 us
    all_to_all x1, starting transfers between devices, from_everyone(): lax.all_to_all(jnp.broadcast_to(x[None], (devices, *x.shape)), axis, 0, 0...  5.71 us
  transfers between devices with their start and end apart: 4, of which 3 were waited for; matrix products, arithmetic and copies ran while one was open for 7% of the time, Pallas kernels for 0%

commit v1 on v0

v1 whole, which is shorter than its diff:
```python
import jax
import jax.numpy as jnp
from jax import lax
from jax.experimental import pallas as pl
from jax.experimental.pallas import tpu as pltpu
from jax.sharding import Mesh
from jax.sharding import PartitionSpec as P

D = 4096
DK = 256
NZ, NX, NY, NC = 8, 4, 4, 2
NJ = NY * NC
ROWS = 32
EPS = 1e-06
MESH = pl.DeviceIdType.MESH
F32 = jnp.float32
BF16 = jnp.bfloat16


def log_sigmoid(v):
    return jnp.minimum(v, 0.0) - jnp.log1p(jnp.exp(-jnp.abs(v)))


def nt(a, b):
    return lax.dot_general(a, b, (((1,), (1,)), ((), ())), preferred_element_type=F32)


def tn(a, b):
    return lax.dot_general(a, b, (((0,), (0,)), ((), ())), preferred_element_type=F32)


def split(v):
    high = v.astype(BF16)
    return high, (v - high.astype(F32)).astype(BF16)


def catch_up_kernel(
    mem_ref, norm_ref, stab_ref, pk_ref, pv_ref, pin_ref, pf_ref, acc_ref,
    mem_out, norm_out, stab_out, mem16_out, norm8_out, coef,
):
    s = pl.program_id(0)

    @pl.when(s == 0)
    def _():
        taken = acc_ref[...]
        stab = stab_ref[...]
        logs, run = [], None
        for j in range(4):
            f = jnp.where(j < taken, log_sigmoid(pf_ref[j]), 0.0)
            run = f if run is None else run + f
            logs.append(run)
        total = run
        ends = [total - logs[j] + pin_ref[j] for j in range(4)]
        new = total + stab
        for j in range(4):
            new = jnp.where(j < taken, jnp.maximum(new, ends[j]), new)
        stab_out[...] = new
        carry = jnp.exp(total + stab - new)
        for j in range(4):
            w = jnp.where(j < taken, jnp.exp(ends[j] - new), 0.0) * (DK**-0.5)
            for h in range(2):
                coef[4 * h + j : 4 * h + j + 1, :] = w[h : h + 1]
        coef[8:10, :] = carry

    lane = lax.broadcasted_iota(jnp.int32, (16, 8), 1)
    col = jnp.sum(jnp.where(lane == s, coef[...], 0.0), axis=1, keepdims=True)
    for h in range(2):
        cols = slice(h * DK, (h + 1) * DK)
        weighted = pk_ref[0, :, cols].astype(F32) * col[4 * h : 4 * h + 4]
        carry = col[8 + h : 9 + h]
        high, low = split(weighted)
        vals = pv_ref[0, :, cols]
        new = carry * mem_ref[0, h] + (tn(high, vals) + tn(low, vals))
        mem_out[0, h] = new
        mem16_out[0, h] = new.astype(BF16)
        row = carry * norm_ref[0, h : h + 1] + jnp.sum(weighted, axis=0, keepdims=True)
        norm_out[0, h : h + 1] = row
        norm8_out[h, pl.ds(s, 1), :] = row


def catch_up(mem, norm, stab_t, pk, pv, pin_t, pf_t, acc):
    whole = lambda *dims: pl.BlockSpec(dims, lambda s: (0,) * len(dims))
    each = lambda *dims: pl.BlockSpec((1, *dims), lambda s: (s,) + (0,) * len(dims))
    return pl.pallas_call(
        catch_up_kernel,
        grid=(8,),
        in_specs=[
            each(2, DK, DK), each(2, DK), whole(2, 8), each(4, 512), each(4, 512),
            whole(4, 2, 8), whole(4, 2, 8), whole(1, 8),
        ],
        out_specs=[
            each(2, DK, DK), each(2, DK), whole(2, 8), each(2, DK, DK), whole(2, 8, DK),
        ],
        out_shape=[
            jax.ShapeDtypeStruct((8, 2, DK, DK), F32),
            jax.ShapeDtypeStruct((8, 2, DK), F32),
            jax.ShapeDtypeStruct((2, 8), F32),
            jax.ShapeDtypeStruct((8, 2, DK, DK), BF16),
            jax.ShapeDtypeStruct((2, 8, DK), F32),
        ],
        scratch_shapes=[pltpu.VMEM((16, 8), F32)],
        name="catch_up",
    )(mem, norm, stab_t, pk, pv, pin_t, pf_t, acc)


def step_kernel(
    tok_ref, gain_ref, wq_ref, wk_ref, wv_ref, wg_ref, gin_ref, gf_ref, bias_ref, wo_ref,
    mem_ref, norm_ref, stab_ref,
    mixed_ref, keys_ref, values_ref,
    wbuf, wob, tok_own, tokbuf, tg, pbuf, rbuf, sbuf, srecv, memv, gin_v, gf_v, gbuf, ebuf, obuf,
    loc_sem, xs_sem, xr_sem, ts_sem, tr_sem, rs_sem, rr_sem, ss_sem, sr_sem, gs_sem, gr_sem,
    es_sem, er_sem,
):
    z, x = lax.axis_index("z"), lax.axis_index("x")
    y, c = lax.axis_index("y"), lax.axis_index("c")
    j = y * NC + c
    right, left = lax.rem(x + 1, NX), lax.rem(x + NX - 1, NX)
    opposite = lax.rem(x + 2, NX)
    zs = [lax.rem(z + d, NZ) for d in range(NZ)]
    js = [lax.rem(j + d, NJ) for d in range(NJ)]
    self_tok = j == z

    def at_x(other):
        return (z, other, y, c)

    def at_z(other):
        return (other, x, y, c)

    def at_zj(other, tp):
        return (other, x, lax.div(tp, NC), lax.rem(tp, NC))

    def rdma(src, dst, ssem, rsem, dev):
        return pltpu.make_async_remote_copy(
            src_ref=src, dst_ref=dst, send_sem=ssem, recv_sem=rsem,
            device_id=dev, device_id_type=MESH,
        )

    def wblock(p, owner, start, size):
        if p < 4:
            first = pl.multiple_of(owner * 128 + start * 128 // 4, 32)
            return wbuf.at[p, pl.ds(first, size * 128 // 4), :]
        cols = pl.ds(pl.multiple_of(owner * 128, 128), 128)
        return wob.at[pl.ds(start * 128, size * 128), cols]

    weights = (wq_ref, wk_ref, wv_ref, wg_ref, wo_ref)
    local = [pltpu.make_async_copy(weights[p], wblock(p, x, 0, 4), loc_sem.at[p]) for p in range(5)]
    local.append(pltpu.make_async_copy(tok_ref, tok_own, loc_sem.at[5]))
    feats = pl.ds(pl.multiple_of(z * 512, 512), 512)
    local.append(pltpu.make_async_copy(gin_ref.at[:, feats], gin_v, loc_sem.at[6]))
    local.append(pltpu.make_async_copy(gf_ref.at[:, feats], gf_v, loc_sem.at[7]))
    local.append(pltpu.make_async_copy(mem_ref, memv, loc_sem.at[8]))
    for copy in local:
        copy.start()

    barrier = pltpu.get_barrier_semaphore()

    def greet(dev):
        pl.semaphore_signal(barrier, inc=1, device_id=dev, device_id_type=MESH)

    greet(at_x(right))
    greet(at_x(left))
    for d in range(1, NZ):
        greet(at_z(zs[d]))
    for d in range(1, NJ):
        greet(at_zj(j, js[d]))
        greet(at_zj(zs[d], z))

    @pl.when(jnp.logical_not(self_tok))
    def _():
        greet(at_zj(j, j))
        greet(at_zj(z, z))

    pl.semaphore_wait(barrier, jnp.where(self_tok, 23, 25))

    def direct(p):
        return [
            rdma(wblock(p, x, 0, 4), wblock(p, x, 0, 4), xs_sem.at[p, 0], xr_sem.at[p, 0], at_x(right)),
            rdma(wblock(p, x, 0, 4), wblock(p, x, 0, 4), xs_sem.at[p, 1], xr_sem.at[p, 1], at_x(left)),
        ]

    def onward(p):
        return [
            rdma(wblock(p, left, 0, 2), wblock(p, left, 0, 2), xs_sem.at[p, 2], xr_sem.at[p, 2], at_x(right)),
            rdma(wblock(p, right, 2, 2), wblock(p, right, 2, 2), xs_sem.at[p, 3], xr_sem.at[p, 3], at_x(left)),
        ]

    def arrive(p, which):
        owner, start, size = ((left, 0, 4), (right, 0, 4), (opposite, 0, 2), (opposite, 2, 2))[which]
        block = wblock(p, owner, start, size)
        rdma(block, block, xs_sem.at[p, which], xr_sem.at[p, which], at_x(left)).wait_recv()

    sent = []

    def go(copies):
        for copy in copies:
            copy.start()
            sent.append(copy)

    local[0].wait()
    go(direct(0))
    local[5].wait()
    tok_copies = [
        rdma(tok_own, tokbuf.at[z], ts_sem.at[d], tr_sem.at[z], at_zj(j, js[d])) for d in range(NJ)
    ]
    go(tok_copies[1:])

    @pl.when(jnp.logical_not(self_tok))
    def _():
        tok_copies[0].start()

    @pl.when(self_tok)
    def _():
        tokbuf[z] = tok_own[...]

    local[1].wait()
    go(direct(1))
    local[2].wait()
    local[3].wait()
    local[4].wait()

    row8 = lax.broadcasted_iota(jnp.int32, (8, 16), 0)
    lane16 = lax.broadcasted_iota(jnp.int32, (8, 16), 1)
    pick_in = jnp.where((row8 < 2) & (lane16 == 2 * j + row8), 1.0, 0.0).astype(BF16)
    pick_f = jnp.where((row8 >= 2) & (row8 < 4) & (lane16 == 2 * j + row8 - 2), 1.0, 0.0).astype(BF16)
    local[6].wait()
    local[7].wait()
    gates8 = (
        jnp.dot(pick_in, gin_v[...], preferred_element_type=F32)
        + jnp.dot(pick_f, gf_v[...], preferred_element_type=F32)
    ).astype(BF16)
    ones8 = jnp.full((8, 512), 1.0, BF16)
    row32 = lax.broadcasted_iota(jnp.int32, (8, ROWS), 0)
    gains = jnp.concatenate([gain_ref[pl.ds(4 * z + r, 1), :] for r in range(4)], axis=1)
    sbuf[...] = jnp.zeros_like(sbuf)

    def token_block(d):
        slot = zs[d]
        if d:
            tok_wait = rdma(tok_own, tokbuf.at[slot], ts_sem.at[d], tr_sem.at[slot], at_zj(slot, z))
            tok_wait.wait_recv()
        else:
            @pl.when(jnp.logical_not(self_tok))
            def _():
                rdma(tok_own, tokbuf.at[slot], ts_sem.at[d], tr_sem.at[slot], at_zj(slot, z)).wait_recv()
        raw = tokbuf[slot].astype(F32)
        scaled = (raw * gains).astype(BF16)
        tg[pl.ds(pl.multiple_of(slot * ROWS, ROWS), ROWS), :] = scaled
        high, low = split(raw * raw)
        squares = nt(ones8, high) + nt(ones8, low)
        sbuf[slot, :, 0:ROWS] = jnp.where(row32 == 4, squares, nt(gates8, scaled))

    for d in (0, 1, 7, 2, 6, 3, 5, 4):
        token_block(d)
    far_first = (4, 3, 5, 2, 6, 1, 7)
    small = [rdma(sbuf.at[zs[d]], srecv.at[d], ss_sem.at[d], sr_sem.at[d], at_z(zs[d])) for d in far_first]
    go(small)

    def project(p):
        part = jnp.dot(tg[...], wbuf[p], preferred_element_type=F32)
        pbuf[p] = part.astype(BF16).reshape(NZ, ROWS, 512)
        go([
            rdma(pbuf.at[p, zs[d]], rbuf.at[p, d], rs_sem.at[p, d], rr_sem.at[p, d], at_z(zs[d]))
            for d in far_first
        ])

    def collect(p):
        total = pbuf[p, z].astype(F32)
        for d in range(1, NZ):
            rdma(pbuf.at[p, zs[d]], rbuf.at[p, d], rs_sem.at[p, d], rr_sem.at[p, d], at_z(zs[d])).wait_recv()
            total = total + rbuf[p, d].astype(F32)
        return total

    for p in range(5):
        arrive(p, 0)
        arrive(p, 1)
        go(onward(p))
        if p + 2 < 5:
            go(direct(p + 2))
        if p >= 1:
            arrive(p - 1, 2)
            arrive(p - 1, 3)
            project(p - 1)

    for copy in small:
        copy.wait_recv()
    sums = sbuf[z]
    for d in range(1, NZ):
        sums = sums + srecv[d]
    scale_row = lax.rsqrt(sums[4:5, 0:ROWS] / D + EPS)
    ri = lax.broadcasted_iota(jnp.int32, (ROWS, ROWS), 0)
    ci = lax.broadcasted_iota(jnp.int32, (ROWS, ROWS), 1)
    eye = ri == ci
    same = lax.div(ri, 4) == lax.div(ci, 4)
    causal = same & (ci <= ri)
    anti = same & (ri <= ci)

    def to_col(row):
        return jnp.sum(jnp.where(eye, row, 0.0), axis=1, keepdims=True)

    scale_col = to_col(scale_row)
    seq_of_row = lax.div(lax.broadcasted_iota(jnp.int32, (ROWS, 8), 0), 4)
    seq_lane = lax.broadcasted_iota(jnp.int32, (ROWS, 8), 1)
    own_seq = seq_of_row == seq_lane
    row_seq = lax.div(lax.broadcasted_iota(jnp.int32, (ROWS, DK), 0), 4)

    local[8].wait()
    query = (collect(0) * scale_col).astype(BF16)
    carried_rows = []
    for h in range(2):
        q = query[:, h * DK : (h + 1) * DK]
        read = jnp.zeros((ROWS, DK), F32)
        for s in range(8):
            part = jnp.dot(q, memv[s, h], preferred_element_type=F32)
            read = jnp.where(row_seq == s, part, read)
        carried_rows.append(read)
    key = (collect(1) * scale_col).astype(BF16)
    keys_ref[...] = key
    value = (collect(2) * scale_col).astype(BF16)
    values_ref[...] = value

    hidden = []
    for h in range(2):
        cols = slice(h * DK, (h + 1) * DK)
        q, k, v = query[:, cols], key[:, cols], value[:, cols]
        in_row = sums[h : h + 1, 0:ROWS] * scale_row
        f_row = log_sigmoid(sums[2 + h : 3 + h, 0:ROWS] * scale_row + bias_ref[2 * j + h])
        f_col = to_col(f_row)
        b_col = jnp.sum(jnp.where(causal, f_row, 0.0), axis=1, keepdims=True)
        b_row = jnp.sum(jnp.where(anti, f_col, 0.0), axis=0, keepdims=True)
        within = jnp.where(causal, b_col - b_row + in_row, -jnp.inf)
        stab_col = jnp.sum(jnp.where(own_seq, stab_ref[h : h + 1, :], 0.0), axis=1, keepdims=True)
        g_col = b_col + stab_col
        level = jnp.maximum(g_col, jnp.max(within, axis=1, keepdims=True))
        u = jnp.exp(g_col - level)
        w = nt(q, k) * (DK**-0.5) * jnp.where(causal, jnp.exp(within - level), 0.0)
        w_high, w_low = split(w)
        n_high, n_low = split(norm_ref[h])
        q_norm = jnp.sum(jnp.where(own_seq, nt(q, n_high) + nt(q, n_low), 0.0), axis=1, keepdims=True)
        num = u * carried_rows[h] + (
            jnp.dot(w_high, v, preferred_element_type=F32) + jnp.dot(w_low, v, preferred_element_type=F32)
        )
        den = u * q_norm + jnp.sum(w, axis=1, keepdims=True)
        hidden.append(num / jnp.maximum(jnp.abs(den), 1.0))

    arrive(4, 2)
    arrive(4, 3)

    gate = jax.nn.sigmoid((collect(3) * scale_col).astype(BF16).astype(F32))
    gbuf[z] = (gate * jnp.concatenate(hidden, axis=1)).astype(BF16)
    go([
        rdma(gbuf.at[z], gbuf.at[z], gs_sem.at[d], gr_sem.at[d], at_z(zs[d])) for d in far_first
    ])

    for d in (0, 1, 7, 2, 6, 3, 5, 4):
        slot = zs[d]
        if d:
            came = NZ - d
            rdma(gbuf.at[slot], gbuf.at[slot], gs_sem.at[came], gr_sem.at[came], at_z(slot)).wait_recv()
        ebuf[slot] = jnp.dot(gbuf[slot], wob[...], preferred_element_type=F32).astype(BF16)
        out = rdma(ebuf.at[slot], obuf.at[j], es_sem.at[d], er_sem.at[j], at_zj(slot, z))
        if d:
            go([out])
        else:
            own_out = out

            @pl.when(jnp.logical_not(self_tok))
            def _():
                own_out.start()

            @pl.when(self_tok)
            def _():
                obuf[j] = ebuf[slot]

    total = None
    for d in range(NJ):
        slot = js[d]
        if d:
            rdma(ebuf.at[0], obuf.at[slot], es_sem.at[d], er_sem.at[slot], at_zj(j, slot)).wait_recv()
        else:
            @pl.when(jnp.logical_not(self_tok))
            def _():
                rdma(ebuf.at[0], obuf.at[slot], es_sem.at[d], er_sem.at[slot], at_zj(j, slot)).wait_recv()
        term = obuf[slot].astype(F32)
        total = term if total is None else total + term
    mixed_ref[...] = total.astype(BF16)

    for copy in sent:
        copy.wait_send()

    @pl.when(jnp.logical_not(self_tok))
    def _():
        tok_copies[0].wait_send()
        own_out.wait_send()


def step(tok, gain, wq, wk, wv, wg, gin_t, gf_t, bias, wo, mem16, norm8, stab_t):
    hbm = pl.BlockSpec(memory_space=pl.ANY)
    vmem = pl.BlockSpec(memory_space=pltpu.VMEM)
    smem = pl.BlockSpec(memory_space=pltpu.SMEM)
    dma = pltpu.SemaphoreType.DMA
    block = lambda *lead: pltpu.VMEM((*lead, ROWS, 512), BF16)
    return pl.pallas_call(
        step_kernel,
        in_specs=[hbm, vmem, hbm, hbm, hbm, hbm, hbm, hbm, smem, hbm, hbm, vmem, vmem],
        out_specs=[vmem, vmem, vmem],
        out_shape=[jax.ShapeDtypeStruct((ROWS, 512), BF16)] * 3,
        scratch_shapes=[
            pltpu.VMEM((4, 512, 512), BF16),
            pltpu.VMEM((512, 512), BF16),
            block(),
            block(NZ),
            pltpu.VMEM((256, 512), BF16),
            block(4, NZ),
            block(4, NZ),
            pltpu.VMEM((NZ, 8, 128), F32),
            pltpu.VMEM((NZ, 8, 128), F32),
            pltpu.VMEM((8, 2, DK, DK), BF16),
            pltpu.VMEM((16, 512), BF16),
            pltpu.VMEM((16, 512), BF16),
            block(NZ),
            block(NZ),
            block(NJ),
            dma((9,)), dma((5, 4)), dma((5, 4)), dma((8,)), dma((8,)), dma((4, 8)), dma((4, 8)),
            dma((8,)), dma((8,)), dma((8,)), dma((8,)), dma((8,)), dma((8,)),
        ],
        compiler_params=pltpu.CompilerParams(
            collective_id=0, has_side_effects=True, vmem_limit_bytes=40 * 1024 * 1024
        ),
        name="step",
    )(tok, gain, wq, wk, wv, wg, gin_t, gf_t, bias, wo, mem16, norm8, stab_t)


def body(
    tokens, norm_gain, query_weight, key_weight, value_weight, outgate_weight, ingate_weight,
    forget_weight, forget_bias, output_weight, state_memory, state_normaliser, state_stabiliser,
    past_keys, past_values, past_ingate, past_forget, accepted,
):
    memory, normaliser, stab_t, mem16, norm8 = catch_up(
        state_memory, state_normaliser, state_stabiliser.T, past_keys, past_values,
        past_ingate.transpose(1, 2, 0), past_forget.transpose(1, 2, 0), accepted.reshape(1, 8),
    )
    mixed, keys, values = step(
        tokens, norm_gain.reshape(32, 128), query_weight, key_weight, value_weight, outgate_weight,
        ingate_weight.T, forget_weight.T, forget_bias, output_weight, mem16, norm8, stab_t,
    )
    return (mixed, memory, normaliser, stab_t.T, keys, values)


def solution(mesh):
    torus = Mesh(mesh.devices.reshape(NZ, NX, NY, NC), ("z", "x", "y", "c"))
    kv, tp = ("z", "x"), ("y", "c")
    in_specs = (
        P(kv, tp), P(), P(kv, tp), P(kv, tp), P(kv, tp), P(kv, tp), P(), P(), P(), P(tp, kv),
        P(kv, tp, None, None), P(kv, tp, None), P(kv, tp), P(kv, None, tp), P(kv, None, tp),
        P(kv, None, tp), P(kv, None, tp), P(kv),
    )
    out_specs = (
        P(kv, tp), P(kv, tp, None, None), P(kv, tp, None), P(kv, tp), P(kv, tp), P(kv, tp),
    )
    return jax.shard_map(body, mesh=torus, in_specs=in_specs, out_specs=out_specs, check_vma=False)
```

time: 219 us -> 91.7 us (0.42); the launches traced: 215 us -> 90.3 us
  waiting for transfers between devices: 108 us -> 0 us
  Pallas kernels: 0 us -> 84.7 us
  blocking collectives: 53.6 us -> 0 us
  matrix products: 16.9 us -> 0 us
  between operations: 14.2 us -> 0.81 us
  local copies, waits for them, and re-layouts: 11.7 us -> 4.87 us
  starting transfers between devices: 5.79 us -> 0 us
  other arithmetic: 4.66 us -> 0 us
    pallas_call x0 -> x2, Pallas kernels: none -> 84.7 us  [the longest x1 76 us: step(): pl.pallas_call(step_kernel, in_specs=[hbm, vmem, hbm, hbm, hbm, hbm, hbm,...]
    unnamed x4 -> x0, waiting for transfers between devices: 52.6 us -> none
    all_gather x1 -> x0, waiting for transfers between devices: 51.2 us -> none  [gathered_by_axis(): nearer = lax.all_gather(x, axes[-1], axis=dim, tiled=True)]
    all_to_all x3 -> x0, blocking collectives: 39.1 us -> none  [the longest x1 22.6 us: body(): blocks = lax.all_to_all(normed, KV, split_axis=1, concat_axis=0, tiled=True)]
    dot_general x12 -> x0, matrix products: 16.9 us -> none  [the longest x1 5.59 us: catch_up(): jnp.einsum('...pd,...pe->...de', weighted, values)]
    all_gather x1 -> x0, blocking collectives: 14.4 us -> none  [gathered_by_axis(): nearer = lax.all_gather(x, axes[-1], axis=dim, tiled=True)]
    all_to_all x1 -> x0, starting transfers between devices: 5.71 us -> none  [from_everyone(): lax.all_to_all(jnp.broadcast_to(x[None], (devices, *x.shape)), axis, 0, 0...]
    all_to_all x1 -> x0, waiting for transfers between devices: 4.31 us -> none  [from_everyone(): lax.all_to_all(jnp.broadcast_to(x[None], (devices, *x.shape)), axis, 0, 0...]
  transfers between devices with their start and end apart: 4 -> 0, of which waited for: 3 -> 0; matrix products, arithmetic and copies ran while one was open for 7% -> 0% of each run, Pallas kernels for 0% -> 0%
where the time goes in v1:
time: 91.7 us; the launch traced here: 90.3 us
  Pallas kernels  84.7 us (92%)
  local copies, waits for them, and re-layouts  4.87 us (5%)
    pallas_call x1, Pallas kernels, step(): pl.pallas_call(step_kernel, in_specs=[hbm, vmem, hbm, hbm, hbm, hbm, hbm,...  76 us
    pallas_call x1, Pallas kernels, catch_up(): pl.pallas_call(catch_up_kernel, grid=(8,), in_specs=[each(2, DK, DK), eac...  8.7 us
    unnamed x29, local copies, waits for them, and re-layouts  4.87 us

profile of v1, /device:TPU:22, one launch (start us, length us, event | category | flops | bytes accessed | tf_op | source)
XLA Modules:
  0.0 90.3 jit_solution(8724707373308638869)
XLA Ops:
  0.6 0.0 copy-start.7
  0.6 0.0 copy-start.12
  0.7 0.0 copy-start.6
  0.7 0.0 copy-start.5
  0.7 0.0 copy-start.4
  0.7 8.7 %catch_up.1 = (f32[8,2,256,256]{3,2,1,0:T(8,128)}, f32[8,2,256]{2,1,0:T(2,128)}, f32[2,8]{1,0:T(2,128)}, bf16[8,2,256,256]{3,2,1,0:T(8,128)(2,1)}, f32[2,8,256]{2,1,0:T(8,128)}) custom-call(f32[8,2,256,256]{3,2,1,0:T(8,128)} %mem_ref.1, f32[8,2,256]{2,1,0:T(2,128)} %norm_ref.1, f32[2,8]{1,0:T(2,128)} %bitcast.14, bf16[8,4,512]{2,1,0:T(4,128)(2,1)} %pk_ref.1, ...), custom_call_target="tpu_custom_call" | custom-call | tf_op jit(solution)/shard_map/catch_up/pallas_call | solution.py:84
  9.4 0.0 copy-done.7
  9.4 0.0 copy-done.12
  9.5 0.0 copy-done.6
  9.5 0.0 copy-done.5
  9.5 0.0 copy-done.4
  9.5 0.0 copy-done.3
  9.5 0.0 copy-done.2
  9.5 0.0 copy-done.1
  9.5 0.0 copy-done.9
  9.5 0.0 copy-done.8
  9.5 0.0 copy-start
  9.5 1.6 %copy-done = bf16[8,2,256,256]{3,2,1,0:T(8,128)(2,1)S(1)} copy-done((bf16[8,2,256,256]{3,2,1,0:T(8,128)(2,1)S(1)}, bf16[8,2,256,256]{3,2,1,0:T(8,128)(2,1)}, u32[]{:S(2)}) %copy-start) | copy-done | bytes 2097176
  11.1 0.7 copy-done.10
  11.8 0.7 copy-done.11
  12.5 76.0 %step.1 = (bf16[32,512]{1,0:T(8,128)(2,1)S(1)}, bf16[32,512]{1,0:T(8,128)(2,1)S(1)}, bf16[32,512]{1,0:T(8,128)(2,1)S(1)}) custom-call(bf16[32,512]{1,0:T(8,128)(2,1)S(1)} %copy-done.8, f32[32,128]{1,0:T(8,128)S(1)} %bitcast.10, bf16[128,512]{1,0:T(8,128)(2,1)S(1)} %copy-done.1, bf16[128,512]{1,0:T(8,128)(2,1)S(1)} %copy-done.2, ...), custom_call_target="tpu_custom_call" | custom-call | tf_op jit(solution)/shard_map/step/pallas_call | solution.py:402
  88.5 0.6 copy.27
  89.1 0.6 copy.28
  89.7 0.6 copy.29
  (7 shorter events, 0.0 us)
Async XLA Ops:
  0.6 8.8 %copy-start.7 = (bf16[512,128]{1,0:T(8,128)(2,1)S(1)}, bf16[512,128]{1,0:T(8,128)(2,1)}, u32[]{:S(2)}) copy-start(bf16[512,128]{1,0:T(8,128)(2,1)} %wo_ref.1) | copy-start | bytes 393220
  0.6 8.8 %copy-start.12 = (f32[16]{0:T(128)S(1)}, f32[16]{0:T(128)}, u32[]{:S(2)}) copy-start(f32[16]{0:T(128)} %bias_ref.1) | copy-start | bytes 196
  0.7 8.8 %copy-start.6 = (bf16[4096,16]{0,1:T(8,128)(2,1)S(1)}, bf16[4096,16]{0,1:T(8,128)(2,1)}, u32[]{:S(2)}) copy-start(bf16[4096,16]{0,1:T(8,128)(2,1)} %param.25) | copy-start | bytes 393220
  0.7 8.8 %copy-start.5 = (bf16[4096,16]{0,1:T(8,128)(2,1)S(1)}, bf16[4096,16]{0,1:T(8,128)(2,1)}, u32[]{:S(2)}) copy-start(bf16[4096,16]{0,1:T(8,128)(2,1)} %param.24) | copy-start | bytes 393220
  0.7 8.8 %copy-start.4 = (bf16[128,512]{1,0:T(8,128)(2,1)S(1)}, bf16[128,512]{1,0:T(8,128)(2,1)}, u32[]{:S(2)}) copy-start(bf16[128,512]{1,0:T(8,128)(2,1)} %wg_ref.1) | copy-start | bytes 393220
  0.7 8.8 %copy-start.3 = (bf16[128,512]{1,0:T(8,128)(2,1)S(1)}, bf16[128,512]{1,0:T(8,128)(2,1)}, u32[]{:S(2)}) copy-start(bf16[128,512]{1,0:T(8,128)(2,1)} %wv_ref.1) | copy-start | bytes 393220
  0.7 8.8 %copy-start.2 = (bf16[128,512]{1,0:T(8,128)(2,1)S(1)}, bf16[128,512]{1,0:T(8,128)(2,1)}, u32[]{:S(2)}) copy-start(bf16[128,512]{1,0:T(8,128)(2,1)} %wk_ref.1) | copy-start | bytes 393220
  0.7 8.8 %copy-start.1 = (bf16[128,512]{1,0:T(8,128)(2,1)S(1)}, bf16[128,512]{1,0:T(8,128)(2,1)}, u32[]{:S(2)}) copy-start(bf16[128,512]{1,0:T(8,128)(2,1)} %wq_ref.1) | copy-start | bytes 393220
  0.7 8.8 %copy-start.9 = (f32[4096]{0:T(1024)S(1)}, f32[4096]{0:T(1024)}, u32[]{:S(2)}) copy-start(f32[4096]{0:T(1024)} %param.19) | copy-start | bytes 49156
  0.7 8.8 %copy-start.8 = (bf16[32,512]{1,0:T(8,128)(2,1)S(1)}, bf16[32,512]{1,0:T(8,128)(2,1)}, u32[]{:S(2)}) copy-start(bf16[32,512]{1,0:T(8,128)(2,1)} %tok_ref.1) | copy-start | bytes 98308
  9.5 1.6 %copy-start = (bf16[8,2,256,256]{3,2,1,0:T(8,128)(2,1)S(1)}, bf16[8,2,256,256]{3,2,1,0:T(8,128)(2,1)}, u32[]{:S(2)}) copy-start(bf16[8,2,256,256]{3,2,1,0:T(8,128)(2,1)} %get-tuple-element.14.mem_ref) | copy-start | bytes 6291460
  11.1 0.7 copy-start.10
  11.8 0.7 copy-start.11

commit v2 on v1

v2 whole, which is shorter than its diff:
```python
import jax
import jax.numpy as jnp
from jax import lax
from jax.experimental import pallas as pl
from jax.experimental.pallas import tpu as pltpu
from jax.sharding import Mesh
from jax.sharding import PartitionSpec as P

D = 4096
DK = 256
NZ, NX, NY, NC = 8, 4, 4, 2
NJ = NY * NC
ROWS = 32
EPS = 1e-06
MESH = pl.DeviceIdType.MESH
F32 = jnp.float32
BF16 = jnp.bfloat16


def log_sigmoid(v):
    return jnp.minimum(v, 0.0) - jnp.log1p(jnp.exp(-jnp.abs(v)))


def nt(a, b):
    return lax.dot_general(a, b, (((1,), (1,)), ((), ())), preferred_element_type=F32)


def tn(a, b):
    return lax.dot_general(a, b, (((0,), (0,)), ((), ())), preferred_element_type=F32)


def split(v):
    high = v.astype(BF16)
    return high, (v - high.astype(F32)).astype(BF16)


def step_kernel(
    tok_ref, gain_ref, wq_ref, wk_ref, wv_ref, wg_ref, gin_ref, gf_ref, bias_ref, wo_ref,
    mem_ref, norm_ref, stab_ref, pk_ref, pv_ref, pin_ref, pf_ref, acc_ref,
    terms_ref, mem_out, norm_out, stab_out, keys_ref, values_ref,
    wbuf, wob, tok_own, tok_mid, tokbuf, tg, pbuf, rbuf, sbuf, srecv, memv, gin_v, gf_v, gbuf, ebuf,
    gain_v, norm_v, stab_v, pk_v, pv_v, pin_v, pf_v, acc_v, bias_v, coef, norm8,
    loc_sem, xs_sem, xr_sem, ys_sem, yr_sem, ts_sem, tr_sem, rs_sem, rr_sem, ss_sem, sr_sem,
    gs_sem, gr_sem, es_sem, er_sem,
):
    z, x = lax.axis_index("z"), lax.axis_index("x")
    y, c = lax.axis_index("y"), lax.axis_index("c")
    j = y * NC + c
    right, left = lax.rem(x + 1, NX), lax.rem(x + NX - 1, NX)
    opposite = lax.rem(x + 2, NX)
    zs = [lax.rem(z + d, NZ) for d in range(NZ)]
    js = [lax.rem(j + d, NJ) for d in range(NJ)]
    ys = [lax.rem(y + d, NY) for d in range(NY)]
    self_tok = j == z

    def at_x(other):
        return (z, other, y, c)

    def at_z(other):
        return (other, x, y, c)

    def at_y(other):
        return (z, x, other, c)

    def at_zj(other, tp):
        return (other, x, lax.div(tp, NC), lax.rem(tp, NC))

    def rdma(src, dst, ssem, rsem, dev):
        return pltpu.make_async_remote_copy(
            src_ref=src, dst_ref=dst, send_sem=ssem, recv_sem=rsem,
            device_id=dev, device_id_type=MESH,
        )

    def wblock(p, owner, start, size):
        if p < 4:
            first = pl.multiple_of(owner * 128 + start * 32, 32)
            return wbuf.at[p, pl.ds(first, size * 32), :]
        cols = pl.ds(pl.multiple_of(owner * 128, 128), 128)
        return wob.at[pl.ds(start * 128, size * 128), cols]

    feats = pl.ds(pl.multiple_of(z * 512, 512), 512)
    moves = (
        (wq_ref, wblock(0, x, 0, 4)), (wk_ref, wblock(1, x, 0, 4)), (wv_ref, wblock(2, x, 0, 4)),
        (wg_ref, wblock(3, x, 0, 4)), (wo_ref, wblock(4, x, 0, 4)), (tok_ref, tok_own),
        (gin_ref.at[:, feats], gin_v), (gf_ref.at[:, feats], gf_v), (mem_ref, mem_out),
        (gain_ref, gain_v), (norm_ref, norm_v), (stab_ref, stab_v), (pk_ref, pk_v), (pv_ref, pv_v),
        (pin_ref, pin_v), (pf_ref, pf_v), (acc_ref, acc_v), (bias_ref, bias_v),
    )
    local = [pltpu.make_async_copy(src, dst, loc_sem.at[i]) for i, (src, dst) in enumerate(moves)]
    for i in (0, 5, 1, 2, 3, 4, 6, 7, 9, 10, 11, 12, 13, 14, 15, 16, 17, 8):
        local[i].start()

    barrier = pltpu.get_barrier_semaphore()

    def greet(dev):
        pl.semaphore_signal(barrier, inc=1, device_id=dev, device_id_type=MESH)

    greet(at_x(right))
    greet(at_x(left))
    for d in range(1, NZ):
        greet(at_z(zs[d]))
        greet((zs[d], x, y, 1 - c))
    for d in range(1, NJ):
        greet(at_zj(z, js[d]))
    pl.semaphore_wait(barrier, 23)

    def direct(p):
        return [
            rdma(wblock(p, x, 0, 4), wblock(p, x, 0, 4), xs_sem.at[p, 0], xr_sem.at[p, 0], at_x(right)),
            rdma(wblock(p, x, 0, 4), wblock(p, x, 0, 4), xs_sem.at[p, 1], xr_sem.at[p, 1], at_x(left)),
        ]

    def onward(p):
        return [
            rdma(wblock(p, left, 0, 2), wblock(p, left, 0, 2), xs_sem.at[p, 2], xr_sem.at[p, 2], at_x(right)),
            rdma(wblock(p, right, 2, 2), wblock(p, right, 2, 2), xs_sem.at[p, 3], xr_sem.at[p, 3], at_x(left)),
        ]

    def arrive(p, which):
        owner, start, size = ((left, 0, 4), (right, 0, 4), (opposite, 0, 2), (opposite, 2, 2))[which]
        block = wblock(p, owner, start, size)
        rdma(block, block, xs_sem.at[p, which], xr_sem.at[p, which], at_x(left)).wait_recv()

    sent = []

    def go(copies):
        for copy in copies:
            copy.start()
            sent.append(copy)

    local[0].wait()
    go(direct(0))
    local[5].wait()
    go([rdma(tok_own, tok_mid.at[y], ys_sem.at[d], yr_sem.at[y], at_y(ys[d])) for d in (2, 1, 3)])
    local[1].wait()
    go(direct(1))

    for i in (11, 14, 15, 16):
        local[i].wait()
    taken = acc_v[...]
    stab = stab_v[...]
    logs, run = [], None
    for i in range(4):
        f = jnp.where(i < taken, log_sigmoid(pf_v[i]), 0.0)
        run = f if run is None else run + f
        logs.append(run)
    ends = [run - logs[i] + pin_v[i] for i in range(4)]
    stab_new = run + stab
    for i in range(4):
        stab_new = jnp.where(i < taken, jnp.maximum(stab_new, ends[i]), stab_new)
    stab_out[...] = stab_new
    for i in range(4):
        w = jnp.where(i < taken, jnp.exp(ends[i] - stab_new), 0.0) * (DK**-0.5)
        for h in range(2):
            coef[4 * h + i : 4 * h + i + 1, :] = w[h : h + 1]
    coef[8:10, :] = jnp.exp(run + stab - stab_new)
    coef[10:16, :] = jnp.zeros((6, 8), F32)
    coef_lane = lax.broadcasted_iota(jnp.int32, (16, 8), 1)
    for i in (8, 10, 12, 13):
        local[i].wait()

    def update(s, carry_in):
        col = jnp.sum(jnp.where(coef_lane == s, coef[...], 0.0), axis=1, keepdims=True)
        for h in range(2):
            cols = slice(h * DK, (h + 1) * DK)
            weighted = pk_v[s, :, cols].astype(F32) * col[4 * h : 4 * h + 4]
            carry = col[8 + h : 9 + h]
            high, low = split(weighted)
            vals = pv_v[s, :, cols]
            new = carry * mem_out[s, h] + (tn(high, vals) + tn(low, vals))
            mem_out[s, h] = new
            memv[s, h] = new.astype(BF16)
            row = carry * norm_v[s, h : h + 1] + jnp.sum(weighted, axis=0, keepdims=True)
            norm_out[s, h : h + 1] = row
            norm8[h, pl.ds(s, 1), :] = row
        return carry_in

    lax.fori_loop(0, 3, update, 0)

    relay_tok = []
    for d in (0, 1, 3, 2):
        far = ys[d] * NC + c
        block = tok_own if d == 0 else tok_mid.at[ys[d]]
        if d:
            rdma(tok_own, block, ys_sem.at[d], yr_sem.at[ys[d]], at_y(ys[d])).wait_recv()
        for core in range(NC):
            copy = rdma(
                block, tokbuf.at[z], ts_sem.at[2 * d + core], tr_sem.at[z],
                (far, x, y, lax.rem(c + core, NC)),
            )
            relay_tok.append((copy, far))

            @pl.when(jnp.logical_not((far == z) & (core == 0)))
            def _(copy=copy):
                copy.start()

        @pl.when(far == z)
        def _(block=block):
            tokbuf[z] = block[...]

    lax.fori_loop(3, 8, update, 0)
    local[2].wait()
    local[3].wait()
    local[4].wait()

    row8 = lax.broadcasted_iota(jnp.int32, (8, 16), 0)
    lane16 = lax.broadcasted_iota(jnp.int32, (8, 16), 1)
    pick_in = jnp.where((row8 < 2) & (lane16 == 2 * j + row8), 1.0, 0.0).astype(BF16)
    pick_f = jnp.where((row8 >= 2) & (row8 < 4) & (lane16 == 2 * j + row8 - 2), 1.0, 0.0).astype(BF16)
    local[6].wait()
    local[7].wait()
    gates8 = (
        jnp.dot(pick_in, gin_v[...], preferred_element_type=F32)
        + jnp.dot(pick_f, gf_v[...], preferred_element_type=F32)
    ).astype(BF16)
    ones8 = jnp.full((8, 512), 1.0, BF16)
    row32 = lax.broadcasted_iota(jnp.int32, (8, ROWS), 0)
    local[9].wait()
    gains = jnp.concatenate([gain_v[pl.ds(4 * z + r, 1), :] for r in range(4)], axis=1)
    sbuf[...] = jnp.zeros_like(sbuf)

    def token_block(d):
        slot = zs[d]
        landed = rdma(tok_own, tokbuf.at[slot], ts_sem.at[d], tr_sem.at[slot], at_z(zs[1]))
        if d:
            landed.wait_recv()
        else:
            @pl.when(lax.rem(z, NC) != c)
            def _():
                landed.wait_recv()
        raw = tokbuf[slot].astype(F32)
        scaled = (raw * gains).astype(BF16)
        tg[pl.ds(pl.multiple_of(slot * ROWS, ROWS), ROWS), :] = scaled
        high, low = split(raw * raw)
        squares = nt(ones8, high) + nt(ones8, low)
        sbuf[slot, :, 0:ROWS] = jnp.where(row32 == 4, squares, nt(gates8, scaled))

    for d in (0, 1, 7, 2, 6, 3, 5, 4):
        token_block(d)
    far_first = (4, 3, 5, 2, 6, 1, 7)
    small = [rdma(sbuf.at[zs[d]], srecv.at[d], ss_sem.at[d], sr_sem.at[d], at_z(zs[d])) for d in far_first]
    go(small)

    def hop(p, block, slot, to):
        return rdma(block, rbuf.at[p, slot], rs_sem.at[p, slot], rr_sem.at[p, slot], at_z(zs[to]))

    def landed(p, slot):
        hop(p, pbuf.at[p, z], slot, 1).wait_recv()
        return rbuf[p, slot].astype(F32)

    def project(p):
        part = jnp.dot(tg[...], wbuf[p], preferred_element_type=F32)
        pbuf[p] = part.astype(BF16).reshape(NZ, ROWS, 512)
        go([
            hop(p, pbuf.at[p, zs[4]], 4, 2 if p % 2 else 6),
            hop(p, pbuf.at[p, zs[3]], 3, 1),
            hop(p, pbuf.at[p, zs[5]], 5, 7),
            hop(p, pbuf.at[p, zs[1]], 1, 1),
            hop(p, pbuf.at[p, zs[7]], 7, 7),
        ])

    def relay(p):
        for to, near in ((2, 3), (6, 5)):
            total = pbuf[p, zs[to]].astype(F32) + landed(p, near)
            if (p % 2 == 0) == (to == 6):
                total = total + landed(p, 4)
            pbuf[p, zs[to]] = total.astype(BF16)
            go([hop(p, pbuf.at[p, zs[to]], to, to)])

    def collect(p):
        total = pbuf[p, z].astype(F32)
        for slot in (1, 7, 2, 6):
            total = total + landed(p, slot)
        return total

    for p in range(4):
        arrive(p, 0)
        arrive(p, 1)
        go(onward(p))
        if p < 2:
            go(direct(p + 2))
        if p == 3:
            go(direct(4))
        if p >= 1:
            arrive(p - 1, 2)
            arrive(p - 1, 3)
            project(p - 1)
        if p >= 2:
            relay(p - 2)
    arrive(3, 2)
    arrive(3, 3)
    project(3)
    relay(2)
    arrive(4, 0)
    arrive(4, 1)
    go(onward(4))

    for copy in small:
        copy.wait_recv()
    sums = sbuf[z]
    for d in range(1, NZ):
        sums = sums + srecv[d]
    scale_row = lax.rsqrt(sums[4:5, 0:ROWS] / D + EPS)
    ri = lax.broadcasted_iota(jnp.int32, (ROWS, ROWS), 0)
    ci = lax.broadcasted_iota(jnp.int32, (ROWS, ROWS), 1)
    eye = ri == ci
    same = lax.div(ri, 4) == lax.div(ci, 4)
    causal = same & (ci <= ri)
    anti = same & (ri <= ci)

    def to_col(row):
        return jnp.sum(jnp.where(eye, row, 0.0), axis=1, keepdims=True)

    scale_col = to_col(scale_row)
    seq_of_row = lax.div(lax.broadcasted_iota(jnp.int32, (ROWS, 8), 0), 4)
    seq_lane = lax.broadcasted_iota(jnp.int32, (ROWS, 8), 1)
    own_seq = seq_of_row == seq_lane
    row_seq = lax.div(lax.broadcasted_iota(jnp.int32, (ROWS, DK), 0), 4)

    query = (collect(0) * scale_col).astype(BF16)
    carried_rows = []
    for h in range(2):
        q = query[:, h * DK : (h + 1) * DK]
        read = jnp.zeros((ROWS, DK), F32)
        for s in range(8):
            part = jnp.dot(q, memv[s, h], preferred_element_type=F32)
            read = jnp.where(row_seq == s, part, read)
        carried_rows.append(read)
    key = (collect(1) * scale_col).astype(BF16)
    keys_ref[...] = key
    value = (collect(2) * scale_col).astype(BF16)
    values_ref[...] = value

    local[17].wait()
    bias_lane = lax.broadcasted_iota(jnp.int32, (1, 16), 1)
    hidden = []
    for h in range(2):
        cols = slice(h * DK, (h + 1) * DK)
        q, k, v = query[:, cols], key[:, cols], value[:, cols]
        bias = jnp.sum(jnp.where(bias_lane == 2 * j + h, bias_v[...], 0.0), axis=1, keepdims=True)
        in_row = sums[h : h + 1, 0:ROWS] * scale_row
        f_row = log_sigmoid(sums[2 + h : 3 + h, 0:ROWS] * scale_row + bias)
        f_col = to_col(f_row)
        b_col = jnp.sum(jnp.where(causal, f_row, 0.0), axis=1, keepdims=True)
        b_row = jnp.sum(jnp.where(anti, f_col, 0.0), axis=0, keepdims=True)
        within = jnp.where(causal, b_col - b_row + in_row, -jnp.inf)
        stab_col = jnp.sum(jnp.where(own_seq, stab_out[h : h + 1, :], 0.0), axis=1, keepdims=True)
        g_col = b_col + stab_col
        level = jnp.maximum(g_col, jnp.max(within, axis=1, keepdims=True))
        u = jnp.exp(g_col - level)
        w = nt(q, k) * (DK**-0.5) * jnp.where(causal, jnp.exp(within - level), 0.0)
        w_high, w_low = split(w)
        n_high, n_low = split(norm8[h])
        q_norm = jnp.sum(jnp.where(own_seq, nt(q, n_high) + nt(q, n_low), 0.0), axis=1, keepdims=True)
        num = u * carried_rows[h] + (
            jnp.dot(w_high, v, preferred_element_type=F32) + jnp.dot(w_low, v, preferred_element_type=F32)
        )
        den = u * q_norm + jnp.sum(w, axis=1, keepdims=True)
        hidden.append(num / jnp.maximum(jnp.abs(den), 1.0))

    relay(3)
    arrive(4, 2)
    arrive(4, 3)

    gate = jax.nn.sigmoid((collect(3) * scale_col).astype(BF16).astype(F32))
    gbuf[z] = (gate * jnp.concatenate(hidden, axis=1)).astype(BF16)
    go([
        rdma(gbuf.at[z], gbuf.at[z], gs_sem.at[d], gr_sem.at[d], at_z(zs[d])) for d in far_first
    ])

    for d in (0, 1, 7, 2, 6, 3, 5, 4):
        slot = zs[d]
        if d:
            came = NZ - d
            rdma(gbuf.at[slot], gbuf.at[slot], gs_sem.at[came], gr_sem.at[came], at_z(slot)).wait_recv()
        ebuf[slot] = jnp.dot(gbuf[slot], wob[...], preferred_element_type=F32).astype(BF16)
        out = rdma(ebuf.at[slot], terms_ref.at[j], es_sem.at[d], er_sem.at[j], at_zj(slot, z))
        if d:
            go([out])
        else:
            own_out = out

            @pl.when(jnp.logical_not(self_tok))
            def _():
                own_out.start()

            @pl.when(self_tok)
            def _():
                terms_ref[j] = ebuf[slot]

    for d in range(NJ):
        slot = js[d]
        came = rdma(ebuf.at[0], terms_ref.at[slot], es_sem.at[d], er_sem.at[slot], at_zj(z, slot))
        if d:
            came.wait_recv()
        else:
            @pl.when(jnp.logical_not(self_tok))
            def _(came=came):
                came.wait_recv()

    for copy in sent:
        copy.wait_send()
    for i, (copy, far) in enumerate(relay_tok):
        @pl.when(jnp.logical_not((far == z) & (i % 2 == 0)))
        def _(copy=copy):
            copy.wait_send()

    @pl.when(jnp.logical_not(self_tok))
    def _():
        own_out.wait_send()


def finish_kernel(terms, mem, norm, stab, keys, values, mixed, mem_o, norm_o, stab_o, keys_o, values_o, sem):
    copy = pltpu.make_async_copy(mem, mem_o, sem)
    copy.start()
    norm_o[...] = norm[...]
    stab_o[...] = stab[...]
    keys_o[...] = keys[...]
    values_o[...] = values[...]
    total = terms[0].astype(F32)
    for i in range(1, NJ):
        total = total + terms[i].astype(F32)
    mixed[...] = total.astype(BF16)
    copy.wait()


def step(*args):
    args = [pltpu.with_memory_space_constraint(a, pltpu.HBM) for a in args]
    hbm = pl.BlockSpec(memory_space=pltpu.HBM)
    vmem = pl.BlockSpec(memory_space=pltpu.VMEM)
    dma = pltpu.SemaphoreType.DMA
    block = lambda *lead: pltpu.VMEM((*lead, ROWS, 512), BF16)
    shape = jax.ShapeDtypeStruct
    outs = [
        shape((NJ, ROWS, 512), BF16), shape((8, 2, DK, DK), F32), shape((8, 2, DK), F32),
        shape((2, 8), F32), shape((ROWS, 512), BF16), shape((ROWS, 512), BF16),
    ]
    parts = pl.pallas_call(
        step_kernel,
        in_specs=[hbm] * 18,
        out_specs=[vmem] * 6,
        out_shape=outs,
        scratch_shapes=[
            pltpu.VMEM((4, 512, 512), BF16),
            pltpu.VMEM((512, 512), BF16),
            block(),
            block(NY),
            block(NZ),
            pltpu.VMEM((256, 512), BF16),
            block(4, NZ),
            block(4, NZ),
            pltpu.VMEM((NZ, 8, 128), F32),
            pltpu.VMEM((NZ, 8, 128), F32),
            pltpu.VMEM((8, 2, DK, DK), BF16),
            pltpu.VMEM((16, 512), BF16),
            pltpu.VMEM((16, 512), BF16),
            block(NZ),
            block(NZ),
            pltpu.VMEM((32, 128), F32),
            pltpu.VMEM((8, 2, DK), F32),
            pltpu.VMEM((2, 8), F32),
            pltpu.VMEM((8, 4, 512), BF16),
            pltpu.VMEM((8, 4, 512), BF16),
            pltpu.VMEM((4, 2, 8), F32),
            pltpu.VMEM((4, 2, 8), F32),
            pltpu.VMEM((1, 8), jnp.int32),
            pltpu.VMEM((1, 16), F32),
            pltpu.VMEM((16, 8), F32),
            pltpu.VMEM((2, 8, DK), F32),
            dma((18,)), dma((5, 4)), dma((5, 4)), dma((4,)), dma((4,)), dma((8,)), dma((8,)),
            dma((4, 8)), dma((4, 8)), dma((8,)), dma((8,)), dma((8,)), dma((8,)), dma((8,)), dma((8,)),
        ],
        compiler_params=pltpu.CompilerParams(
            collective_id=0, has_side_effects=True, vmem_limit_bytes=24 * 1024 * 1024
        ),
        name="step",
    )(*args)
    return pl.pallas_call(
        finish_kernel,
        in_specs=[vmem, pl.BlockSpec(memory_space=pl.ANY), vmem, vmem, vmem, vmem],
        out_specs=[vmem, hbm, vmem, vmem, vmem, vmem],
        out_shape=[shape((ROWS, 512), BF16)] + outs[1:],
        scratch_shapes=[dma],
        name="finish",
        compiler_params=pltpu.CompilerParams(vmem_limit_bytes=4 * 1024 * 1024),
    )(*[pltpu.with_memory_space_constraint(part, pltpu.VMEM) for part in parts])


def body(
    tokens, norm_gain, query_weight, key_weight, value_weight, outgate_weight, ingate_weight,
    forget_weight, forget_bias, output_weight, state_memory, state_normaliser, state_stabiliser,
    past_keys, past_values, past_ingate, past_forget, accepted,
):
    mixed, memory, normaliser, stab_t, keys, values = step(
        tokens, norm_gain.reshape(32, 128), query_weight, key_weight, value_weight, outgate_weight,
        ingate_weight.T, forget_weight.T, forget_bias.reshape(1, 16), output_weight,
        state_memory, state_normaliser, state_stabiliser.T, past_keys, past_values,
        past_ingate.transpose(1, 2, 0), past_forget.transpose(1, 2, 0), accepted.reshape(1, 8),
    )
    return (mixed, memory, normaliser, stab_t.T, keys, values)


def solution(mesh):
    torus = Mesh(mesh.devices.reshape(NZ, NX, NY, NC), ("z", "x", "y", "c"))
    kv, tp = ("z", "x"), ("y", "c")
    in_specs = (
        P(kv, tp), P(), P(kv, tp), P(kv, tp), P(kv, tp), P(kv, tp), P(), P(), P(), P(tp, kv),
        P(kv, tp, None, None), P(kv, tp, None), P(kv, tp), P(kv, None, tp), P(kv, None, tp),
        P(kv, None, tp), P(kv, None, tp), P(kv),
    )
    out_specs = (
        P(kv, tp), P(kv, tp, None, None), P(kv, tp, None), P(kv, tp), P(kv, tp), P(kv, tp),
    )
    return jax.shard_map(body, mesh=torus, in_specs=in_specs, out_specs=out_specs, check_vma=False)
```

time: 91.7 us -> 68.4 us (0.75)
  Pallas kernels: 84.7 us -> 67.2 us
  local copies, waits for them, and re-layouts: 4.87 us -> 0 us
    pallas_call x2, Pallas kernels: 84.7 us -> 67.2 us  [the longest x1 64.5 us: step(): pl.pallas_call(step_kernel, in_specs=[hbm] * 18, out_specs=[vmem] * 6, ou...]
    unnamed x29 -> x0, local copies, waits for them, and re-layouts: 4.87 us -> none
where the time goes in v2:
time: 68.4 us; the launch traced here: 67.8 us
  Pallas kernels  67.2 us (98%)
    pallas_call x1, Pallas kernels, step(): pl.pallas_call(step_kernel, in_specs=[hbm] * 18, out_specs=[vmem] * 6, ou...  64.5 us
    pallas_call x1, Pallas kernels, step(): pl.pallas_call(finish_kernel, in_specs=[vmem, pl.BlockSpec(memory_space=p...  2.67 us

profile of v2, /device:TPU:22, one launch (start us, length us, event | category | flops | bytes accessed | tf_op | source)
XLA Modules:
  0.0 67.8 jit_solution(10080242315884947763)
XLA Ops:
  0.6 64.5 %step.1 = (bf16[8,32,512]{2,1,0:T(8,128)(2,1)S(1)}, f32[8,2,256,256]{3,2,1,0:T(8,128)S(1)}, f32[8,2,256]{2,1,0:T(2,128)S(1)}, f32[2,8]{1,0:T(2,128)S(1)}, bf16[3...) custom-call(bf16[32,512]{1,0:T(8,128)(2,1)} %tok_ref.1, f32[32,128]{1,0:T(8,128)} %bitcast.11, ...), custom_call_target="tpu_custom_call" | custom-call | tf_op jit(solution)/shard_map/step/pallas_call | solution.py:438
  65.2 2.7 %finish.1 = (bf16[32,512]{1,0:T(8,128)(2,1)}, f32[8,2,256,256]{3,2,1,0:T(8,128)}, f32[8,2,256]{2,1,0:T(2,128)}, f32[2,8]{1,0:T(2,128)}, bf16[32,512]{1,0:T(8,128)(2,1)}, /*index=5*/bf16[32,512]{1,0:T(8,128)(2,1)}) custom-call(bf16[8,32,512]{2,1,0:T(8,128)(2,1)S(1)} %get-tuple-element.18.terms, f32[8,2,256,256]{3,2,1,0:T(8,128)S(1)} %get-tuple-element.19.mem, ...), custom_call_target="tpu_custom_call" | custom-call | tf_op jit(solution)/shard_map/finish/pallas_call | solution.py:478

commit v3 on v2

--- a/solution.py
+++ b/solution.py
@@ -12,6 +12,7 @@
 NJ = NY * NC
 ROWS = 32
 EPS = 1e-06
+RELAYED = 6
 MESH = pl.DeviceIdType.MESH
 F32 = jnp.float32
 BF16 = jnp.bfloat16
@@ -72,7 +73,7 @@
         )
 
     def wblock(p, owner, start, size):
-        if p < 4:
+        if p < 8:
             first = pl.multiple_of(owner * 128 + start * 32, 32)
             return wbuf.at[p, pl.ds(first, size * 32), :]
         cols = pl.ds(pl.multiple_of(owner * 128, 128), 128)
@@ -80,14 +81,17 @@
 
     feats = pl.ds(pl.multiple_of(z * 512, 512), 512)
     moves = (
-        (wq_ref, wblock(0, x, 0, 4)), (wk_ref, wblock(1, x, 0, 4)), (wv_ref, wblock(2, x, 0, 4)),
-        (wg_ref, wblock(3, x, 0, 4)), (wo_ref, wblock(4, x, 0, 4)), (tok_ref, tok_own),
-        (gin_ref.at[:, feats], gin_v), (gf_ref.at[:, feats], gf_v), (mem_ref, mem_out),
+        *(
+            (w.at[:, pl.ds(h * DK, DK)], wblock(2 * i + h, x, 0, 4))
+            for i, w in enumerate((wq_ref, wk_ref, wv_ref, wg_ref))
+            for h in range(2)
+        ),
+        (wo_ref, wblock(8, x, 0, 4)), (tok_ref, tok_own), (gin_ref.at[:, feats], gin_v), (gf_ref.at[:, feats], gf_v), (mem_ref, mem_out),
         (gain_ref, gain_v), (norm_ref, norm_v), (stab_ref, stab_v), (pk_ref, pk_v), (pv_ref, pv_v),
         (pin_ref, pin_v), (pf_ref, pf_v), (acc_ref, acc_v), (bias_ref, bias_v),
     )
     local = [pltpu.make_async_copy(src, dst, loc_sem.at[i]) for i, (src, dst) in enumerate(moves)]
-    for i in (0, 5, 1, 2, 3, 4, 6, 7, 9, 10, 11, 12, 13, 14, 15, 16, 17, 8):
+    for i in (0, 9, 1, 2, 3, 4, 5, 6, 7, 15, 18, 19, 20, 13, 14, 16, 17, 10, 11, 21, 8, 12):
         local[i].start()
 
     barrier = pltpu.get_barrier_semaphore()
@@ -128,14 +132,23 @@
             copy.start()
             sent.append(copy)
 
+    def forward(p):
+        arrive(p, 0)
+        arrive(p, 1)
+        go(onward(p))
+        if p < 5:
+            local[p + 3].wait()
+            go(direct(p + 3))
+
     local[0].wait()
     go(direct(0))
-    local[5].wait()
+    local[9].wait()
     go([rdma(tok_own, tok_mid.at[y], ys_sem.at[d], yr_sem.at[y], at_y(ys[d])) for d in (2, 1, 3)])
-    local[1].wait()
-    go(direct(1))
-
-    for i in (11, 14, 15, 16):
+    for p in (1, 2):
+        local[p].wait()
+        go(direct(p))
+
+    for i in (15, 18, 19, 20):
         local[i].wait()
     taken = acc_v[...]
     stab = stab_v[...]
@@ -156,7 +169,7 @@
     coef[8:10, :] = jnp.exp(run + stab - stab_new)
     coef[10:16, :] = jnp.zeros((6, 8), F32)
     coef_lane = lax.broadcasted_iota(jnp.int32, (16, 8), 1)
-    for i in (8, 10, 12, 13):
+    for i in (12, 14, 16, 17):
         local[i].wait()
 
     def update(s, carry_in):
@@ -175,7 +188,8 @@
             norm8[h, pl.ds(s, 1), :] = row
         return carry_in
 
-    lax.fori_loop(0, 3, update, 0)
+    forward(0)
+    lax.fori_loop(0, 1, update, 0)
 
     relay_tok = []
     for d in (0, 1, 3, 2):
@@ -198,24 +212,24 @@
         def _(block=block):
             tokbuf[z] = block[...]
 
-    lax.fori_loop(3, 8, update, 0)
-    local[2].wait()
-    local[3].wait()
-    local[4].wait()
-
+    forward(1)
+    lax.fori_loop(1, 4, update, 0)
+    forward(2)
+    lax.fori_loop(4, 8, update, 0)
+    forward(3)
     row8 = lax.broadcasted_iota(jnp.int32, (8, 16), 0)
     lane16 = lax.broadcasted_iota(jnp.int32, (8, 16), 1)
     pick_in = jnp.where((row8 < 2) & (lane16 == 2 * j + row8), 1.0, 0.0).astype(BF16)
     pick_f = jnp.where((row8 >= 2) & (row8 < 4) & (lane16 == 2 * j + row8 - 2), 1.0, 0.0).astype(BF16)
-    local[6].wait()
-    local[7].wait()
+    local[10].wait()
+    local[11].wait()
     gates8 = (
         jnp.dot(pick_in, gin_v[...], preferred_element_type=F32)
         + jnp.dot(pick_f, gf_v[...], preferred_element_type=F32)
     ).astype(BF16)
     ones8 = jnp.full((8, 512), 1.0, BF16)
     row32 = lax.broadcasted_iota(jnp.int32, (8, ROWS), 0)
-    local[9].wait()
+    local[13].wait()
     gains = jnp.concatenate([gain_v[pl.ds(4 * z + r, 1), :] for r in range(4)], axis=1)
     sbuf[...] = jnp.zeros_like(sbuf)
 
@@ -249,15 +263,20 @@
         return rbuf[p, slot].astype(F32)
 
     def project(p):
+        arrive(p, 2)
+        arrive(p, 3)
         part = jnp.dot(tg[...], wbuf[p], preferred_element_type=F32)
-        pbuf[p] = part.astype(BF16).reshape(NZ, ROWS, 512)
-        go([
-            hop(p, pbuf.at[p, zs[4]], 4, 2 if p % 2 else 6),
-            hop(p, pbuf.at[p, zs[3]], 3, 1),
-            hop(p, pbuf.at[p, zs[5]], 5, 7),
-            hop(p, pbuf.at[p, zs[1]], 1, 1),
-            hop(p, pbuf.at[p, zs[7]], 7, 7),
-        ])
+        pbuf[p] = part.astype(BF16).reshape(NZ, ROWS, DK)
+        if p < RELAYED:
+            go([
+                hop(p, pbuf.at[p, zs[4]], 4, 2 if p % 2 else 6),
+                hop(p, pbuf.at[p, zs[3]], 3, 1),
+                hop(p, pbuf.at[p, zs[5]], 5, 7),
+                hop(p, pbuf.at[p, zs[1]], 1, 1),
+                hop(p, pbuf.at[p, zs[7]], 7, 7),
+            ])
+        else:
+            go([hop(p, pbuf.at[p, zs[d]], d, d) for d in far_first])
 
     def relay(p):
         for to, near in ((2, 3), (6, 5)):
@@ -269,31 +288,21 @@
 
     def collect(p):
         total = pbuf[p, z].astype(F32)
-        for slot in (1, 7, 2, 6):
+        for slot in (1, 7, 2, 6) if p < RELAYED else (1, 7, 2, 6, 3, 5, 4):
             total = total + landed(p, slot)
-        return total
-
-    for p in range(4):
-        arrive(p, 0)
-        arrive(p, 1)
-        go(onward(p))
-        if p < 2:
-            go(direct(p + 2))
+        return (total * scale_col).astype(BF16)
+
+    for p in range(8):
+        if p < 4:
+            forward(p + 4)
         if p == 3:
-            go(direct(4))
-        if p >= 1:
-            arrive(p - 1, 2)
-            arrive(p - 1, 3)
-            project(p - 1)
-        if p >= 2:
-            relay(p - 2)
-    arrive(3, 2)
-    arrive(3, 3)
-    project(3)
-    relay(2)
-    arrive(4, 0)
-    arrive(4, 1)
-    go(onward(4))
+            local[8].wait()
+            go(direct(8))
+        project(p)
+        if 0 <= p - 3 < RELAYED:
+            relay(p - 3)
+    for p in range(5, RELAYED):
+        relay(p)
 
     for copy in small:
         copy.wait_recv()
@@ -317,26 +326,27 @@
     own_seq = seq_of_row == seq_lane
     row_seq = lax.div(lax.broadcasted_iota(jnp.int32, (ROWS, DK), 0), 4)
 
-    query = (collect(0) * scale_col).astype(BF16)
-    carried_rows = []
+    queries, keys, values, carried_rows = [], [], [], []
     for h in range(2):
-        q = query[:, h * DK : (h + 1) * DK]
+        q = collect(h)
+        queries.append(q)
         read = jnp.zeros((ROWS, DK), F32)
         for s in range(8):
             part = jnp.dot(q, memv[s, h], preferred_element_type=F32)
             read = jnp.where(row_seq == s, part, read)
         carried_rows.append(read)
-    key = (collect(1) * scale_col).astype(BF16)
-    keys_ref[...] = key
-    value = (collect(2) * scale_col).astype(BF16)
-    values_ref[...] = value
-
-    local[17].wait()
+    for h in range(2):
+        keys.append(collect(2 + h))
+        keys_ref[:, h * DK : (h + 1) * DK] = keys[h]
+    for h in range(2):
+        values.append(collect(4 + h))
+        values_ref[:, h * DK : (h + 1) * DK] = values[h]
+
+    local[21].wait()
     bias_lane = lax.broadcasted_iota(jnp.int32, (1, 16), 1)
     hidden = []
     for h in range(2):
-        cols = slice(h * DK, (h + 1) * DK)
-        q, k, v = query[:, cols], key[:, cols], value[:, cols]
+        q, k, v = queries[h], keys[h], values[h]
         bias = jnp.sum(jnp.where(bias_lane == 2 * j + h, bias_v[...], 0.0), axis=1, keepdims=True)
         in_row = sums[h : h + 1, 0:ROWS] * scale_row
         f_row = log_sigmoid(sums[2 + h : 3 + h, 0:ROWS] * scale_row + bias)
@@ -358,22 +368,30 @@
         den = u * q_norm + jnp.sum(w, axis=1, keepdims=True)
         hidden.append(num / jnp.maximum(jnp.abs(den), 1.0))
 
-    relay(3)
-    arrive(4, 2)
-    arrive(4, 3)
-
-    gate = jax.nn.sigmoid((collect(3) * scale_col).astype(BF16).astype(F32))
-    gbuf[z] = (gate * jnp.concatenate(hidden, axis=1)).astype(BF16)
-    go([
-        rdma(gbuf.at[z], gbuf.at[z], gs_sem.at[d], gr_sem.at[d], at_z(zs[d])) for d in far_first
-    ])
+    arrive(8, 0)
+    arrive(8, 1)
+    go(onward(8))
+    for h in range(2):
+        gate = jax.nn.sigmoid(collect(6 + h).astype(F32))
+        gbuf[h, z] = (gate * hidden[h]).astype(BF16)
+        go([
+            rdma(gbuf.at[h, z], gbuf.at[h, z], gs_sem.at[h, d], gr_sem.at[h, d], at_z(zs[d]))
+            for d in far_first
+        ])
+    arrive(8, 2)
+    arrive(8, 3)
 
     for d in (0, 1, 7, 2, 6, 3, 5, 4):
         slot = zs[d]
-        if d:
-            came = NZ - d
-            rdma(gbuf.at[slot], gbuf.at[slot], gs_sem.at[came], gr_sem.at[came], at_z(slot)).wait_recv()
-        ebuf[slot] = jnp.dot(gbuf[slot], wob[...], preferred_element_type=F32).astype(BF16)
+        out = jnp.zeros((ROWS, 512), F32)
+        for h in range(2):
+            if d:
+                came = NZ - d
+                rdma(
+                    gbuf.at[h, slot], gbuf.at[h, slot], gs_sem.at[h, came], gr_sem.at[h, came], at_z(slot)
+                ).wait_recv()
+            out = out + jnp.dot(gbuf[h, slot], wob[h * DK : (h + 1) * DK, :], preferred_element_type=F32)
+        ebuf[slot] = out.astype(BF16)
         out = rdma(ebuf.at[slot], terms_ref.at[j], es_sem.at[d], er_sem.at[j], at_zj(slot, z))
         if d:
             go([out])
@@ -410,18 +428,19 @@
         own_out.wait_send()
 
 
-def finish_kernel(terms, mem, norm, stab, keys, values, mixed, mem_o, norm_o, stab_o, keys_o, values_o, sem):
-    copy = pltpu.make_async_copy(mem, mem_o, sem)
-    copy.start()
-    norm_o[...] = norm[...]
-    stab_o[...] = stab[...]
-    keys_o[...] = keys[...]
-    values_o[...] = values[...]
+def finish_kernel(terms, mem, norm, stab, keys, values, mixed, mem_o, norm_o, stab_o, keys_o, values_o, total_v, sem):
+    pairs = ((mem, mem_o), (norm, norm_o), (stab, stab_o), (keys, keys_o), (values, values_o), (total_v, mixed))
+    copies = [pltpu.make_async_copy(src, dst, sem.at[i]) for i, (src, dst) in enumerate(pairs)]
+    for copy in copies[1:5]:
+        copy.start()
     total = terms[0].astype(F32)
     for i in range(1, NJ):
         total = total + terms[i].astype(F32)
-    mixed[...] = total.astype(BF16)
-    copy.wait()
+    total_v[...] = total.astype(BF16)
+    copies[0].start()
+    copies[5].start()
+    for copy in copies:
+        copy.wait()
 
 
 def step(*args):
@@ -441,20 +460,20 @@
         out_specs=[vmem] * 6,
         out_shape=outs,
         scratch_shapes=[
-            pltpu.VMEM((4, 512, 512), BF16),
+            pltpu.VMEM((8, 512, DK), BF16),
             pltpu.VMEM((512, 512), BF16),
             block(),
             block(NY),
             block(NZ),
             pltpu.VMEM((256, 512), BF16),
-            block(4, NZ),
-            block(4, NZ),
+            pltpu.VMEM((8, NZ, ROWS, DK), BF16),
+            pltpu.VMEM((8, NZ, ROWS, DK), BF16),
             pltpu.VMEM((NZ, 8, 128), F32),
             pltpu.VMEM((NZ, 8, 128), F32),
             pltpu.VMEM((8, 2, DK, DK), BF16),
             pltpu.VMEM((16, 512), BF16),
             pltpu.VMEM((16, 512), BF16),
-            block(NZ),
+            pltpu.VMEM((2, NZ, ROWS, DK), BF16),
             block(NZ),
             pltpu.VMEM((32, 128), F32),
             pltpu.VMEM((8, 2, DK), F32),
@@ -467,8 +486,8 @@
             pltpu.VMEM((1, 16), F32),
             pltpu.VMEM((16, 8), F32),
             pltpu.VMEM((2, 8, DK), F32),
-            dma((18,)), dma((5, 4)), dma((5, 4)), dma((4,)), dma((4,)), dma((8,)), dma((8,)),
-            dma((4, 8)), dma((4, 8)), dma((8,)), dma((8,)), dma((8,)), dma((8,)), dma((8,)), dma((8,)),
+            dma((22,)), dma((9, 4)), dma((9, 4)), dma((4,)), dma((4,)), dma((8,)), dma((8,)),
+            dma((8, 8)), dma((8, 8)), dma((8,)), dma((8,)), dma((2, 8)), dma((2, 8)), dma((8,)), dma((8,)),
         ],
         compiler_params=pltpu.CompilerParams(
             collective_id=0, has_side_effects=True, vmem_limit_bytes=24 * 1024 * 1024
@@ -477,10 +496,10 @@
     )(*args)
     return pl.pallas_call(
         finish_kernel,
-        in_specs=[vmem, pl.BlockSpec(memory_space=pl.ANY), vmem, vmem, vmem, vmem],
-        out_specs=[vmem, hbm, vmem, vmem, vmem, vmem],
+        in_specs=[vmem] + [pl.BlockSpec(memory_space=pl.ANY)] * 5,
+        out_specs=[hbm] * 6,
         out_shape=[shape((ROWS, 512), BF16)] + outs[1:],
-        scratch_shapes=[dma],
+        scratch_shapes=[pltpu.VMEM((ROWS, 512), BF16), dma((6,))],
         name="finish",
         compiler_params=pltpu.CompilerParams(vmem_limit_bytes=4 * 1024 * 1024),
     )(*[pltpu.with_memory_space_constraint(part, pltpu.VMEM) for part in parts])

time: 68.4 us -> 64 us (0.936)
  the two profiles are of different devices: /device:TPU:22 before, /device:TPU:51 now
where the time goes in v3:
time: 64 us; the launch traced here: 63.9 us
  Pallas kernels  63.2 us (99%)
  between operations  0.65 us (1%)
    pallas_call x1, Pallas kernels, step(): pl.pallas_call(step_kernel, in_specs=[hbm] * 18, out_specs=[vmem] * 6, ou...  61.1 us
    pallas_call x1, Pallas kernels, step(): pl.pallas_call(finish_kernel, in_specs=[vmem] + [pl.BlockSpec(memory_spac...  2.11 us

profile of v3, /device:TPU:51, one launch (start us, length us, event | category | flops | bytes accessed | tf_op | source)
XLA Modules:
  0.0 63.9 jit_solution(636302591883434696)
XLA Ops:
  0.6 61.1 %step.1 = (bf16[8,32,512]{2,1,0:T(8,128)(2,1)S(1)}, f32[8,2,256,256]{3,2,1,0:T(8,128)S(1)}, f32[8,2,256]{2,1,0:T(2,128)S(1)}, f32[2,8]{1,0:T(2,128)S(1)}, bf16[3...) custom-call(bf16[32,512]{1,0:T(8,128)(2,1)} %tok_ref.1, f32[32,128]{1,0:T(8,128)} %bitcast.11, ...), custom_call_target="tpu_custom_call" | custom-call | tf_op jit(solution)/shard_map/step/pallas_call | solution.py:457
  61.8 2.1 %finish.1 = (bf16[32,512]{1,0:T(8,128)(2,1)}, f32[8,2,256,256]{3,2,1,0:T(8,128)}, f32[8,2,256]{2,1,0:T(2,128)}, f32[2,8]{1,0:T(2,128)}, bf16[32,512]{1,0:T(8,128)(2,1)}, /*index=5*/bf16[32,512]{1,0:T(8,128)(2,1)}) custom-call(bf16[8,32,512]{2,1,0:T(8,128)(2,1)S(1)} %get-tuple-element.18.terms, f32[8,2,256,256]{3,2,1,0:T(8,128)S(1)} %get-tuple-element.19.mem, ...), custom_call_target="tpu_custom_call" | custom-call | tf_op jit(solution)/shard_map/finish/pallas_call | solution.py:497

commit v4 on v3

--- a/solution.py
+++ b/solution.py
@@ -12,7 +12,8 @@
 NJ = NY * NC
 ROWS = 32
 EPS = 1e-06
-RELAYED = 6
+MODES = (2, 2, 2, 2, 2, 2, 2, 2)
+ORDER = "P0 P1 F6 P2 P3 F7 D B0 P4 B1 P5 B2 S P6 B3 P7 B4 B5 B6 B7"
 MESH = pl.DeviceIdType.MESH
 F32 = jnp.float32
 BF16 = jnp.bfloat16
@@ -189,7 +190,6 @@
         return carry_in
 
     forward(0)
-    lax.fori_loop(0, 1, update, 0)
 
     relay_tok = []
     for d in (0, 1, 3, 2):
@@ -213,25 +213,15 @@
             tokbuf[z] = block[...]
 
     forward(1)
-    lax.fori_loop(1, 4, update, 0)
+    lax.fori_loop(0, 2, update, 0)
     forward(2)
-    lax.fori_loop(4, 8, update, 0)
+    lax.fori_loop(2, 4, update, 0)
     forward(3)
-    row8 = lax.broadcasted_iota(jnp.int32, (8, 16), 0)
-    lane16 = lax.broadcasted_iota(jnp.int32, (8, 16), 1)
-    pick_in = jnp.where((row8 < 2) & (lane16 == 2 * j + row8), 1.0, 0.0).astype(BF16)
-    pick_f = jnp.where((row8 >= 2) & (row8 < 4) & (lane16 == 2 * j + row8 - 2), 1.0, 0.0).astype(BF16)
-    local[10].wait()
-    local[11].wait()
-    gates8 = (
-        jnp.dot(pick_in, gin_v[...], preferred_element_type=F32)
-        + jnp.dot(pick_f, gf_v[...], preferred_element_type=F32)
-    ).astype(BF16)
-    ones8 = jnp.full((8, 512), 1.0, BF16)
-    row32 = lax.broadcasted_iota(jnp.int32, (8, ROWS), 0)
+    lax.fori_loop(4, 6, update, 0)
+    forward(4)
+    lax.fori_loop(6, 8, update, 0)
     local[13].wait()
     gains = jnp.concatenate([gain_v[pl.ds(4 * z + r, 1), :] for r in range(4)], axis=1)
-    sbuf[...] = jnp.zeros_like(sbuf)
 
     def token_block(d):
         slot = zs[d]
@@ -242,19 +232,15 @@
             @pl.when(lax.rem(z, NC) != c)
             def _():
                 landed.wait_recv()
-        raw = tokbuf[slot].astype(F32)
-        scaled = (raw * gains).astype(BF16)
+        scaled = (tokbuf[slot].astype(F32) * gains).astype(BF16)
         tg[pl.ds(pl.multiple_of(slot * ROWS, ROWS), ROWS), :] = scaled
-        high, low = split(raw * raw)
-        squares = nt(ones8, high) + nt(ones8, low)
-        sbuf[slot, :, 0:ROWS] = jnp.where(row32 == 4, squares, nt(gates8, scaled))
-
-    for d in (0, 1, 7, 2, 6, 3, 5, 4):
+
+    for d in (0, 1, 7, 2, 6):
+        token_block(d)
+    forward(5)
+    for d in (3, 5, 4):
         token_block(d)
     far_first = (4, 3, 5, 2, 6, 1, 7)
-    small = [rdma(sbuf.at[zs[d]], srecv.at[d], ss_sem.at[d], sr_sem.at[d], at_z(zs[d])) for d in far_first]
-    go(small)
-
     def hop(p, block, slot, to):
         return rdma(block, rbuf.at[p, slot], rs_sem.at[p, slot], rr_sem.at[p, slot], at_z(zs[to]))
 
@@ -267,42 +253,74 @@
         arrive(p, 3)
         part = jnp.dot(tg[...], wbuf[p], preferred_element_type=F32)
         pbuf[p] = part.astype(BF16).reshape(NZ, ROWS, DK)
-        if p < RELAYED:
-            go([
-                hop(p, pbuf.at[p, zs[4]], 4, 2 if p % 2 else 6),
-                hop(p, pbuf.at[p, zs[3]], 3, 1),
-                hop(p, pbuf.at[p, zs[5]], 5, 7),
-                hop(p, pbuf.at[p, zs[1]], 1, 1),
-                hop(p, pbuf.at[p, zs[7]], 7, 7),
-            ])
-        else:
+        if MODES[p] == 1:
             go([hop(p, pbuf.at[p, zs[d]], d, d) for d in far_first])
+            return
+        go([
+            hop(p, pbuf.at[p, zs[4]], 4, 2 if p % 2 else 6),
+            hop(p, pbuf.at[p, zs[3]], 3, 1),
+            hop(p, pbuf.at[p, zs[5]], 5, 7),
+        ])
+        if MODES[p] == 2:
+            go([hop(p, pbuf.at[p, zs[1]], 1, 1), hop(p, pbuf.at[p, zs[7]], 7, 7)])
+
+    def pass_on(p, target, via, terms):
+        total = pbuf[p, zs[target]].astype(F32)
+        for slot in terms:
+            total = total + landed(p, slot)
+        pbuf[p, zs[target]] = total.astype(BF16)
+        go([hop(p, pbuf.at[p, zs[target]], target, via)])
 
     def relay(p):
-        for to, near in ((2, 3), (6, 5)):
-            total = pbuf[p, zs[to]].astype(F32) + landed(p, near)
-            if (p % 2 == 0) == (to == 6):
-                total = total + landed(p, 4)
-            pbuf[p, zs[to]] = total.astype(BF16)
-            go([hop(p, pbuf.at[p, zs[to]], to, to)])
+        far = MODES[p] == 2
+        pass_on(p, 2, 2 if far else 1, (3, 4) if p % 2 else (3,))
+        pass_on(p, 6, 6 if far else 7, (5,) if p % 2 else (5, 4))
+
+    def relay_near(p):
+        pass_on(p, 1, 1, (2,))
+        pass_on(p, 7, 7, (6,))
 
     def collect(p):
         total = pbuf[p, z].astype(F32)
-        for slot in (1, 7, 2, 6) if p < RELAYED else (1, 7, 2, 6, 3, 5, 4):
+        for slot in ((1, 7, 2, 6, 3, 5, 4), (1, 7, 2, 6), (1, 7))[MODES[p] - 1]:
             total = total + landed(p, slot)
         return (total * scale_col).astype(BF16)
 
-    for p in range(8):
-        if p < 4:
-            forward(p + 4)
-        if p == 3:
+    small = []
+
+    def send_small():
+        row8 = lax.broadcasted_iota(jnp.int32, (8, 16), 0)
+        lane16 = lax.broadcasted_iota(jnp.int32, (8, 16), 1)
+        pick_in = jnp.where((row8 < 2) & (lane16 == 2 * j + row8), 1.0, 0.0).astype(BF16)
+        pick_f = jnp.where((row8 >= 2) & (row8 < 4) & (lane16 == 2 * j + row8 - 2), 1.0, 0.0).astype(BF16)
+        local[10].wait()
+        local[11].wait()
+        gates8 = (
+            jnp.dot(pick_in, gin_v[...], preferred_element_type=F32)
+            + jnp.dot(pick_f, gf_v[...], preferred_element_type=F32)
+        ).astype(BF16)
+        ones8 = jnp.full((8, 512), 1.0, BF16)
+        row_all = lax.broadcasted_iota(jnp.int32, (8, NZ * ROWS), 0)
+        sbuf[...] = jnp.zeros_like(sbuf)
+        raw = tokbuf[...].astype(F32).reshape(NZ * ROWS, 512)
+        high, low = split(raw * raw)
+        squares = nt(ones8, high) + nt(ones8, low)
+        rows = jnp.where(row_all == 4, squares, nt(gates8, tg[...]))
+        for i in range(NZ):
+            sbuf[i, :, 0:ROWS] = rows[:, i * ROWS : (i + 1) * ROWS]
+        small.extend(
+            rdma(sbuf.at[zs[d]], srecv.at[d], ss_sem.at[d], sr_sem.at[d], at_z(zs[d])) for d in far_first
+        )
+        go(small)
+
+    for op in ORDER.split():
+        if op == "S":
+            send_small()
+        elif op == "D":
             local[8].wait()
             go(direct(8))
-        project(p)
-        if 0 <= p - 3 < RELAYED:
-            relay(p - 3)
-    for p in range(5, RELAYED):
-        relay(p)
+        else:
+            {"P": project, "B": relay, "C": relay_near, "F": forward}[op[0]](int(op[1]))
 
     for copy in small:
         copy.wait_recv()

time: 64 us -> 60.8 us (0.950)
  the two profiles are of different devices: /device:TPU:51 before, /device:TPU:22 now
where the time goes in v4:
time: 60.8 us; the launch traced here: 60.7 us
  Pallas kernels  60 us (99%)
  between operations  0.65 us (1%)
    pallas_call x1, Pallas kernels, step(): pl.pallas_call(step_kernel, in_specs=[hbm] * 18, out_specs=[vmem] * 6, ou...  57.9 us
    pallas_call x1, Pallas kernels, step(): pl.pallas_call(finish_kernel, in_specs=[vmem] + [pl.BlockSpec(memory_spac...  2.11 us

profile of v4, /device:TPU:22, one launch (start us, length us, event | category | flops | bytes accessed | tf_op | source)
XLA Modules:
  0.0 60.7 jit_solution(2237108932150657985)
XLA Ops:
  0.6 57.9 %step.1 = (bf16[8,32,512]{2,1,0:T(8,128)(2,1)S(1)}, f32[8,2,256,256]{3,2,1,0:T(8,128)S(1)}, f32[8,2,256]{2,1,0:T(2,128)S(1)}, f32[2,8]{1,0:T(2,128)S(1)}, bf16[3...) custom-call(bf16[32,512]{1,0:T(8,128)(2,1)} %tok_ref.1, f32[32,128]{1,0:T(8,128)} %bitcast.11, ...), custom_call_target="tpu_custom_call" | custom-call | tf_op jit(solution)/shard_map/step/pallas_call | solution.py:475
  58.6 2.1 %finish.1 = (bf16[32,512]{1,0:T(8,128)(2,1)}, f32[8,2,256,256]{3,2,1,0:T(8,128)}, f32[8,2,256]{2,1,0:T(2,128)}, f32[2,8]{1,0:T(2,128)}, bf16[32,512]{1,0:T(8,128)(2,1)}, /*index=5*/bf16[32,512]{1,0:T(8,128)(2,1)}) custom-call(bf16[8,32,512]{2,1,0:T(8,128)(2,1)S(1)} %get-tuple-element.18.terms, f32[8,2,256,256]{3,2,1,0:T(8,128)S(1)} %get-tuple-element.19.mem, ...), custom_call_target="tpu_custom_call" | custom-call | tf_op jit(solution)/shard_map/finish/pallas_call | solution.py:515

commit v5 on v4

--- a/solution.py
+++ b/solution.py
@@ -12,8 +12,8 @@
 NJ = NY * NC
 ROWS = 32
 EPS = 1e-06
-MODES = (2, 2, 2, 2, 2, 2, 2, 2)
-ORDER = "P0 P1 F6 P2 P3 F7 D B0 P4 B1 P5 B2 S P6 B3 P7 B4 B5 B6 B7"
+RELAYED = 3
+PIECES = ((0, True), (1, True), (2, True), (0, False), (1, False), (2, False), (3, True), (3, False))
 MESH = pl.DeviceIdType.MESH
 F32 = jnp.float32
 BF16 = jnp.bfloat16
@@ -40,9 +40,9 @@
     tok_ref, gain_ref, wq_ref, wk_ref, wv_ref, wg_ref, gin_ref, gf_ref, bias_ref, wo_ref,
     mem_ref, norm_ref, stab_ref, pk_ref, pv_ref, pin_ref, pf_ref, acc_ref,
     terms_ref, mem_out, norm_out, stab_out, keys_ref, values_ref,
-    wbuf, wob, tok_own, tok_mid, tokbuf, tg, pbuf, rbuf, sbuf, srecv, memv, gin_v, gf_v, gbuf, ebuf,
+    wbuf, swap, wob, tok_own, tok_mid, tokbuf, tg, pbuf, rbuf, sbuf, srecv, memv, gin_v, gf_v, gbuf, ebuf,
     gain_v, norm_v, stab_v, pk_v, pv_v, pin_v, pf_v, acc_v, bias_v, coef, norm8,
-    loc_sem, xs_sem, xr_sem, ys_sem, yr_sem, ts_sem, tr_sem, rs_sem, rr_sem, ss_sem, sr_sem,
+    loc_sem, xs_sem, xr_sem, ws_sem, wr_sem, fs_sem, fr_sem, ys_sem, yr_sem, ts_sem, tr_sem, rs_sem, rr_sem, ss_sem, sr_sem,
     gs_sem, gr_sem, es_sem, er_sem,
 ):
     z, x = lax.axis_index("z"), lax.axis_index("x")
@@ -54,6 +54,10 @@
     js = [lax.rem(j + d, NJ) for d in range(NJ)]
     ys = [lax.rem(y + d, NY) for d in range(NY)]
     self_tok = j == z
+    even = lax.rem(z, 2)
+    odd = 1 - even
+    partner = z + 1 - 2 * even
+    base = z - even
 
     def at_x(other):
         return (z, other, y, c)
@@ -73,26 +77,29 @@
             device_id=dev, device_id_type=MESH,
         )
 
-    def wblock(p, owner, start, size):
-        if p < 8:
+    own_cols = pl.ds(pl.multiple_of(even * DK, DK), DK)
+    other_cols = pl.ds(pl.multiple_of(odd * DK, DK), DK)
+
+    def wblock(piece, owner, start, size):
+        if piece < 8:
+            proj, own = PIECES[piece]
             first = pl.multiple_of(owner * 128 + start * 32, 32)
-            return wbuf.at[p, pl.ds(first, size * 32), :]
+            return wbuf.at[proj, even if own else odd, pl.ds(first, size * 32), :]
         cols = pl.ds(pl.multiple_of(owner * 128, 128), 128)
         return wob.at[pl.ds(start * 128, size * 128), cols]
 
     feats = pl.ds(pl.multiple_of(z * 512, 512), 512)
     moves = (
-        *(
-            (w.at[:, pl.ds(h * DK, DK)], wblock(2 * i + h, x, 0, 4))
-            for i, w in enumerate((wq_ref, wk_ref, wv_ref, wg_ref))
-            for h in range(2)
-        ),
+        (wq_ref.at[:, own_cols], wblock(0, x, 0, 4)), (wk_ref.at[:, own_cols], wblock(1, x, 0, 4)),
+        (wv_ref.at[:, own_cols], wblock(2, x, 0, 4)), (wg_ref.at[:, own_cols], wblock(6, x, 0, 4)),
+        (wq_ref.at[:, other_cols], swap.at[0]), (wk_ref.at[:, other_cols], swap.at[1]),
+        (wv_ref.at[:, other_cols], swap.at[2]), (wg_ref.at[:, other_cols], swap.at[3]),
         (wo_ref, wblock(8, x, 0, 4)), (tok_ref, tok_own), (gin_ref.at[:, feats], gin_v), (gf_ref.at[:, feats], gf_v), (mem_ref, mem_out),
         (gain_ref, gain_v), (norm_ref, norm_v), (stab_ref, stab_v), (pk_ref, pk_v), (pv_ref, pv_v),
         (pin_ref, pin_v), (pf_ref, pf_v), (acc_ref, acc_v), (bias_ref, bias_v),
     )
     local = [pltpu.make_async_copy(src, dst, loc_sem.at[i]) for i, (src, dst) in enumerate(moves)]
-    for i in (0, 9, 1, 2, 3, 4, 5, 6, 7, 15, 18, 19, 20, 13, 14, 16, 17, 10, 11, 21, 8, 12):
+    for i in (0, 9, 4, 1, 2, 5, 6, 7, 3, 15, 18, 19, 20, 13, 14, 16, 17, 10, 11, 21, 8, 12):
         local[i].start()
 
     barrier = pltpu.get_barrier_semaphore()
@@ -133,21 +140,57 @@
             copy.start()
             sent.append(copy)
 
+    def give(proj):
+        mine = wbuf.at[proj, even, pl.ds(pl.multiple_of(x * 128, 128), 128), :]
+        return rdma(swap.at[proj], mine, ws_sem.at[proj], wr_sem.at[proj], at_z(partner))
+
+    def send(piece):
+        if piece < 8:
+            proj, own = PIECES[piece]
+            if own:
+                local[proj].wait()
+            else:
+                block = wblock(piece, x, 0, 4)
+                rdma(swap.at[proj], block, ws_sem.at[proj], wr_sem.at[proj], at_z(partner)).wait_recv()
+        else:
+            local[8].wait()
+        go(direct(piece))
+
     def forward(p):
         arrive(p, 0)
         arrive(p, 1)
         go(onward(p))
         if p < 5:
-            local[p + 3].wait()
-            go(direct(p + 3))
-
-    local[0].wait()
-    go(direct(0))
+            send(p + 3)
+
+    send(0)
     local[9].wait()
     go([rdma(tok_own, tok_mid.at[y], ys_sem.at[d], yr_sem.at[y], at_y(ys[d])) for d in (2, 1, 3)])
-    for p in (1, 2):
-        local[p].wait()
-        go(direct(p))
+    relay_tok = []
+
+    def spread(d):
+        block = tok_own if d == 0 else tok_mid.at[ys[d]]
+        if d:
+            rdma(tok_own, block, ys_sem.at[d], yr_sem.at[ys[d]], at_y(ys[d])).wait_recv()
+        same, cross = 2 * ys[d] + even, 2 * ys[d] + odd
+        first = rdma(block, tokbuf.at[c, z], ts_sem.at[2 * d], tr_sem.at[z], at_z(same))
+        go([rdma(block, tokbuf.at[c, z], ts_sem.at[2 * d + 1], tr_sem.at[z], at_z(cross))])
+        relay_tok.append((first, same))
+
+        @pl.when(same != z)
+        def _():
+            first.start()
+
+        @pl.when(same == z)
+        def _():
+            tokbuf[c, z] = block[...]
+
+    spread(0)
+    for proj in range(4):
+        local[4 + proj].wait()
+        go([give(proj)])
+        if proj < 2:
+            send(proj + 1)
 
     for i in (15, 18, 19, 20):
         local[i].wait()
@@ -191,26 +234,8 @@
 
     forward(0)
 
-    relay_tok = []
-    for d in (0, 1, 3, 2):
-        far = ys[d] * NC + c
-        block = tok_own if d == 0 else tok_mid.at[ys[d]]
-        if d:
-            rdma(tok_own, block, ys_sem.at[d], yr_sem.at[ys[d]], at_y(ys[d])).wait_recv()
-        for core in range(NC):
-            copy = rdma(
-                block, tokbuf.at[z], ts_sem.at[2 * d + core], tr_sem.at[z],
-                (far, x, y, lax.rem(c + core, NC)),
-            )
-            relay_tok.append((copy, far))
-
-            @pl.when(jnp.logical_not((far == z) & (core == 0)))
-            def _(copy=copy):
-                copy.start()
-
-        @pl.when(far == z)
-        def _(block=block):
-            tokbuf[z] = block[...]
+    for d in (1, 3, 2):
+        spread(d)
 
     forward(1)
     lax.fori_loop(0, 2, update, 0)
@@ -221,25 +246,33 @@
     forward(4)
     lax.fori_loop(6, 8, update, 0)
     local[13].wait()
-    gains = jnp.concatenate([gain_v[pl.ds(4 * z + r, 1), :] for r in range(4)], axis=1)
-
-    def token_block(d):
+
+    def gains_of(plane):
+        rows = [gain_v[pl.ds(4 * (base + plane) + r, 1), :] for r in range(4)]
+        return jnp.concatenate(rows, axis=1)
+
+    def crossing(core, slot):
+        block = tokbuf.at[core, slot]
+        return rdma(block, block, fs_sem.at[slot], fr_sem.at[slot], (z, x, y, 1 - c))
+
+    def scale_block(core, slot, gains):
+        scaled = (tokbuf[core, slot].astype(F32) * gains).astype(BF16)
+        tg[core, pl.ds(pl.multiple_of(slot * ROWS, ROWS), ROWS), :] = scaled
+
+    near_first = (0, 1, 7, 2, 6, 3, 5, 4)
+    own_gains = gains_of(c)
+    for d in near_first:
         slot = zs[d]
-        landed = rdma(tok_own, tokbuf.at[slot], ts_sem.at[d], tr_sem.at[slot], at_z(zs[1]))
         if d:
-            landed.wait_recv()
-        else:
-            @pl.when(lax.rem(z, NC) != c)
-            def _():
-                landed.wait_recv()
-        scaled = (tokbuf[slot].astype(F32) * gains).astype(BF16)
-        tg[pl.ds(pl.multiple_of(slot * ROWS, ROWS), ROWS), :] = scaled
-
-    for d in (0, 1, 7, 2, 6):
-        token_block(d)
+            rdma(tok_own, tokbuf.at[c, slot], ts_sem.at[0], tr_sem.at[slot], at_z(slot)).wait_recv()
+        go([crossing(c, slot)])
+        scale_block(c, slot, own_gains)
     forward(5)
-    for d in (3, 5, 4):
-        token_block(d)
+    other_gains = gains_of(1 - c)
+    for d in near_first:
+        slot = zs[d]
+        crossing(1 - c, slot).wait_recv()
+        scale_block(1 - c, slot, other_gains)
     far_first = (4, 3, 5, 2, 6, 1, 7)
     def hop(p, block, slot, to):
         return rdma(block, rbuf.at[p, slot], rs_sem.at[p, slot], rr_sem.at[p, slot], at_z(zs[to]))
@@ -249,42 +282,44 @@
         return rbuf[p, slot].astype(F32)
 
     def project(p):
-        arrive(p, 2)
-        arrive(p, 3)
-        part = jnp.dot(tg[...], wbuf[p], preferred_element_type=F32)
+        for piece in range(8):
+            if PIECES[piece][0] == p:
+                arrive(piece, 2)
+                arrive(piece, 3)
+        part = jnp.dot(tg[0], wbuf[p, 0], preferred_element_type=F32)
+        part = part + jnp.dot(tg[1], wbuf[p, 1], preferred_element_type=F32)
         pbuf[p] = part.astype(BF16).reshape(NZ, ROWS, DK)
-        if MODES[p] == 1:
+        if p >= RELAYED:
             go([hop(p, pbuf.at[p, zs[d]], d, d) for d in far_first])
             return
+        ahead, back = (2, 6) if p % 2 == 0 else (6, 2)
         go([
-            hop(p, pbuf.at[p, zs[4]], 4, 2 if p % 2 else 6),
-            hop(p, pbuf.at[p, zs[3]], 3, 1),
-            hop(p, pbuf.at[p, zs[5]], 5, 7),
+            hop(p, pbuf.at[p, zs[4]], 4, ahead),
+            hop(p, pbuf.at[p, zs[3]], 3, 2),
+            hop(p, pbuf.at[p, zs[5]], 5, 6),
+            hop(p, pbuf.at[p, zs[back]], back, back),
         ])
-        if MODES[p] == 2:
-            go([hop(p, pbuf.at[p, zs[1]], 1, 1), hop(p, pbuf.at[p, zs[7]], 7, 7)])
-
-    def pass_on(p, target, via, terms):
-        total = pbuf[p, zs[target]].astype(F32)
-        for slot in terms:
-            total = total + landed(p, slot)
+
+    def pass_on(p, target, slot):
+        total = pbuf[p, zs[target]].astype(F32) + landed(p, slot)
         pbuf[p, zs[target]] = total.astype(BF16)
-        go([hop(p, pbuf.at[p, zs[target]], target, via)])
+        go([hop(p, pbuf.at[p, zs[target]], target, target)])
 
     def relay(p):
-        far = MODES[p] == 2
-        pass_on(p, 2, 2 if far else 1, (3, 4) if p % 2 else (3,))
-        pass_on(p, 6, 6 if far else 7, (5,) if p % 2 else (5, 4))
-
-    def relay_near(p):
-        pass_on(p, 1, 1, (2,))
-        pass_on(p, 7, 7, (6,))
+        pass_on(p, 1, 3)
+        pass_on(p, 7, 5)
+        pass_on(p, 2 if p % 2 == 0 else 6, 4)
 
     def collect(p):
-        total = pbuf[p, z].astype(F32)
-        for slot in ((1, 7, 2, 6, 3, 5, 4), (1, 7, 2, 6), (1, 7))[MODES[p] - 1]:
-            total = total + landed(p, slot)
-        return (total * scale_col).astype(BF16)
+        mine = pbuf[p, z].astype(F32)
+        for slot in (2, 6) if p < RELAYED else (2, 6, 4):
+            mine = mine + landed(p, slot)
+        other = landed(p, 1)
+        for slot in (7,) if p < RELAYED else (7, 3, 5):
+            other = other + landed(p, slot)
+        mine = (mine * scale_col).astype(BF16)
+        other = (other * scale_col).astype(BF16)
+        return jnp.where(even == 0, mine, other), jnp.where(even == 0, other, mine)
 
     small = []
 
@@ -302,10 +337,10 @@
         ones8 = jnp.full((8, 512), 1.0, BF16)
         row_all = lax.broadcasted_iota(jnp.int32, (8, NZ * ROWS), 0)
         sbuf[...] = jnp.zeros_like(sbuf)
-        raw = tokbuf[...].astype(F32).reshape(NZ * ROWS, 512)
+        raw = tokbuf[even].astype(F32).reshape(NZ * ROWS, 512)
         high, low = split(raw * raw)
         squares = nt(ones8, high) + nt(ones8, low)
-        rows = jnp.where(row_all == 4, squares, nt(gates8, tg[...]))
+        rows = jnp.where(row_all == 4, squares, nt(gates8, tg[even]))
         for i in range(NZ):
             sbuf[i, :, 0:ROWS] = rows[:, i * ROWS : (i + 1) * ROWS]
         small.extend(
@@ -313,14 +348,17 @@
         )
         go(small)
 
-    for op in ORDER.split():
-        if op == "S":
-            send_small()
-        elif op == "D":
-            local[8].wait()
-            go(direct(8))
-        else:
-            {"P": project, "B": relay, "C": relay_near, "F": forward}[op[0]](int(op[1]))
+    project(0)
+    forward(6)
+    project(1)
+    forward(7)
+    send(8)
+    project(2)
+    send_small()
+    relay(0)
+    relay(1)
+    project(3)
+    relay(2)
 
     for copy in small:
         copy.wait_recv()
@@ -344,20 +382,18 @@
     own_seq = seq_of_row == seq_lane
     row_seq = lax.div(lax.broadcasted_iota(jnp.int32, (ROWS, DK), 0), 4)
 
-    queries, keys, values, carried_rows = [], [], [], []
+    queries = collect(0)
+    carried_rows = []
     for h in range(2):
-        q = collect(h)
-        queries.append(q)
         read = jnp.zeros((ROWS, DK), F32)
         for s in range(8):
-            part = jnp.dot(q, memv[s, h], preferred_element_type=F32)
+            part = jnp.dot(queries[h], memv[s, h], preferred_element_type=F32)
             read = jnp.where(row_seq == s, part, read)
         carried_rows.append(read)
+    keys = collect(1)
+    values = collect(2)
     for h in range(2):
-        keys.append(collect(2 + h))
         keys_ref[:, h * DK : (h + 1) * DK] = keys[h]
-    for h in range(2):
-        values.append(collect(4 + h))
         values_ref[:, h * DK : (h + 1) * DK] = values[h]
 
     local[21].wait()
@@ -389,9 +425,10 @@
     arrive(8, 0)
     arrive(8, 1)
     go(onward(8))
+    pre = collect(3)
     for h in range(2):
-        gate = jax.nn.sigmoid(collect(6 + h).astype(F32))
-        gbuf[h, z] = (gate * hidden[h]).astype(BF16)
+        gbuf[h, z] = (jax.nn.sigmoid(pre[h].astype(F32)) * hidden[h]).astype(BF16)
+    for h in range(2):
         go([
             rdma(gbuf.at[h, z], gbuf.at[h, z], gs_sem.at[h, d], gr_sem.at[h, d], at_z(zs[d]))
             for d in far_first
@@ -436,8 +473,8 @@
 
     for copy in sent:
         copy.wait_send()
-    for i, (copy, far) in enumerate(relay_tok):
-        @pl.when(jnp.logical_not((far == z) & (i % 2 == 0)))
+    for copy, same in relay_tok:
+        @pl.when(same != z)
         def _(copy=copy):
             copy.wait_send()
 
@@ -478,14 +515,15 @@
         out_specs=[vmem] * 6,
         out_shape=outs,
         scratch_shapes=[
-            pltpu.VMEM((8, 512, DK), BF16),
+            pltpu.VMEM((4, 2, 512, DK), BF16),
+            pltpu.VMEM((4, 128, DK), BF16),
             pltpu.VMEM((512, 512), BF16),
             block(),
             block(NY),
-            block(NZ),
-            pltpu.VMEM((256, 512), BF16),
-            pltpu.VMEM((8, NZ, ROWS, DK), BF16),
-            pltpu.VMEM((8, NZ, ROWS, DK), BF16),
+            block(2, NZ),
+            pltpu.VMEM((2, 256, 512), BF16),
+            pltpu.VMEM((4, NZ, ROWS, DK), BF16),
+            pltpu.VMEM((4, NZ, ROWS, DK), BF16),
             pltpu.VMEM((NZ, 8, 128), F32),
             pltpu.VMEM((NZ, 8, 128), F32),
             pltpu.VMEM((8, 2, DK, DK), BF16),
@@ -505,7 +543,8 @@
             pltpu.VMEM((16, 8), F32),
             pltpu.VMEM((2, 8, DK), F32),
             dma((22,)), dma((9, 4)), dma((9, 4)), dma((4,)), dma((4,)), dma((8,)), dma((8,)),
-            dma((8, 8)), dma((8, 8)), dma((8,)), dma((8,)), dma((2, 8)), dma((2, 8)), dma((8,)), dma((8,)),
+            dma((4,)), dma((4,)), dma((8,)), dma((8,)),
+            dma((4, 8)), dma((4, 8)), dma((8,)), dma((8,)), dma((2, 8)), dma((2, 8)), dma((8,)), dma((8,)),
         ],
         compiler_params=pltpu.CompilerParams(
             collective_id=0, has_side_effects=True, vmem_limit_bytes=24 * 1024 * 1024

time: 60.8 us -> 59 us (0.970)
  Pallas kernels: 60 us -> 57.8 us
    pallas_call x1, Pallas kernels: 57.9 us -> 55.7 us  [step(): pl.pallas_call(step_kernel, in_specs=[hbm] * 18, out_specs=[vmem] * 6, ou...]
where the time goes in v5:
time: 59 us; the launch traced here: 58.5 us
  Pallas kernels  57.8 us (98%)
  between operations  0.65 us (1%)
    pallas_call x1, Pallas kernels, step(): pl.pallas_call(step_kernel, in_specs=[hbm] * 18, out_specs=[vmem] * 6, ou...  55.7 us
    pallas_call x1, Pallas kernels, step(): pl.pallas_call(finish_kernel, in_specs=[vmem] + [pl.BlockSpec(memory_spac...  2.11 us

profile of v5, /device:TPU:22, one launch (start us, length us, event | category | flops | bytes accessed | tf_op | source)
XLA Modules:
  0.0 58.5 jit_solution(11915225620044597048)
XLA Ops:
  0.6 55.7 %step.1 = (bf16[8,32,512]{2,1,0:T(8,128)(2,1)S(1)}, f32[8,2,256,256]{3,2,1,0:T(8,128)S(1)}, f32[8,2,256]{2,1,0:T(2,128)S(1)}, f32[2,8]{1,0:T(2,128)S(1)}, bf16[3...) custom-call(bf16[32,512]{1,0:T(8,128)(2,1)} %tok_ref.1, f32[32,128]{1,0:T(8,128)} %bitcast.11, ...), custom_call_target="tpu_custom_call" | custom-call | tf_op jit(solution)/shard_map/step/pallas_call | solution.py:512
  56.4 2.1 %finish.1 = (bf16[32,512]{1,0:T(8,128)(2,1)}, f32[8,2,256,256]{3,2,1,0:T(8,128)}, f32[8,2,256]{2,1,0:T(2,128)}, f32[2,8]{1,0:T(2,128)}, bf16[32,512]{1,0:T(8,128)(2,1)}, /*index=5*/bf16[32,512]{1,0:T(8,128)(2,1)}) custom-call(bf16[8,32,512]{2,1,0:T(8,128)(2,1)S(1)} %get-tuple-element.18.terms, f32[8,2,256,256]{3,2,1,0:T(8,128)S(1)} %get-tuple-element.19.mem, ...), custom_call_target="tpu_custom_call" | custom-call | tf_op jit(solution)/shard_map/finish/pallas_call | solution.py:554

commit v6 on v5

--- a/solution.py
+++ b/solution.py
@@ -12,7 +12,7 @@
 NJ = NY * NC
 ROWS = 32
 EPS = 1e-06
-RELAYED = 3
+RELAYED = 2
 PIECES = ((0, True), (1, True), (2, True), (0, False), (1, False), (2, False), (3, True), (3, False))
 MESH = pl.DeviceIdType.MESH
 F32 = jnp.float32
@@ -354,11 +354,10 @@
     forward(7)
     send(8)
     project(2)
+    relay(0)
     send_small()
-    relay(0)
     relay(1)
     project(3)
-    relay(2)
 
     for copy in small:
         copy.wait_recv()
@@ -428,15 +427,15 @@
     pre = collect(3)
     for h in range(2):
         gbuf[h, z] = (jax.nn.sigmoid(pre[h].astype(F32)) * hidden[h]).astype(BF16)
-    for h in range(2):
-        go([
-            rdma(gbuf.at[h, z], gbuf.at[h, z], gs_sem.at[h, d], gr_sem.at[h, d], at_z(zs[d]))
-            for d in far_first
-        ])
+    go([
+        rdma(gbuf.at[h, z], gbuf.at[h, z], gs_sem.at[h, d], gr_sem.at[h, d], at_z(zs[d]))
+        for d in far_first
+        for h in range(2)
+    ])
     arrive(8, 2)
     arrive(8, 3)
 
-    for d in (0, 1, 7, 2, 6, 3, 5, 4):
+    for d in (3, 5, 1, 7, 2, 6, 4, 0):
         slot = zs[d]
         out = jnp.zeros((ROWS, 512), F32)
         for h in range(2):

time: 59 us -> 57.9 us (0.981)
  Pallas kernels: 57.8 us -> 57.1 us
    pallas_call x1, Pallas kernels: 55.7 us -> 55 us  [step(): pl.pallas_call(step_kernel, in_specs=[hbm] * 18, out_specs=[vmem] * 6, ou...]
where the time goes in v6:
time: 57.9 us; the launch traced here: 57.7 us
  Pallas kernels  57.1 us (99%)
  between operations  0.65 us (1%)
    pallas_call x1, Pallas kernels, step(): pl.pallas_call(step_kernel, in_specs=[hbm] * 18, out_specs=[vmem] * 6, ou...  55 us
    pallas_call x1, Pallas kernels, step(): pl.pallas_call(finish_kernel, in_specs=[vmem] + [pl.BlockSpec(memory_spac...  2.11 us

profile of v6, /device:TPU:22, one launch (start us, length us, event | category | flops | bytes accessed | tf_op | source)
XLA Modules:
  0.0 57.7 jit_solution(16131324720153361735)
XLA Ops:
  0.6 55.0 %step.1 = (bf16[8,32,512]{2,1,0:T(8,128)(2,1)S(1)}, f32[8,2,256,256]{3,2,1,0:T(8,128)S(1)}, f32[8,2,256]{2,1,0:T(2,128)S(1)}, f32[2,8]{1,0:T(2,128)S(1)}, bf16[3...) custom-call(bf16[32,512]{1,0:T(8,128)(2,1)} %tok_ref.1, f32[32,128]{1,0:T(8,128)} %bitcast.11, ...), custom_call_target="tpu_custom_call" | custom-call | tf_op jit(solution)/shard_map/step/pallas_call | solution.py:511
  55.6 2.1 %finish.1 = (bf16[32,512]{1,0:T(8,128)(2,1)}, f32[8,2,256,256]{3,2,1,0:T(8,128)}, f32[8,2,256]{2,1,0:T(2,128)}, f32[2,8]{1,0:T(2,128)}, bf16[32,512]{1,0:T(8,128)(2,1)}, /*index=5*/bf16[32,512]{1,0:T(8,128)(2,1)}) custom-call(bf16[8,32,512]{2,1,0:T(8,128)(2,1)S(1)} %get-tuple-element.18.terms, f32[8,2,256,256]{3,2,1,0:T(8,128)S(1)} %get-tuple-element.19.mem, ...), custom_call_target="tpu_custom_call" | custom-call | tf_op jit(solution)/shard_map/finish/pallas_call | solution.py:553
